TPU v7x, 32 devices: a whole 2x2x4 slice. The times are simulated.
32 devices in a mesh: grp: 2 (over y), ep: 8 (over z, core), tp: 2 (over x).
Axes of the slice: x: 2, y: 2, z: 4, core: 2. Of those that a mesh axis runs over, the one named last changes fastest.
Arguments:
- tokens: bfloat16 [512, 2048], P(('grp', 'ep')), parts along dimension 0, may hold values from -12 to 12
- routes: int32 [512, 4], P(('grp', 'ep')), parts along dimension 0, may hold values from 0 to 7, all different within a row; in each aligned block of 32 rows (0 to 31, 32 to 63, ...) at most 32 rows name the same one
- gates: float32 [512, 4], P(('grp', 'ep')), parts along dimension 0, may hold values from 0.1 to 1
- norm_gain: bfloat16 [2048], replicated, may hold values from 0.099609375 to 1.8984375
- exp_gate: bfloat16 [8, 2048, 2048], P('ep', None, 'tp'), may hold values from -0.125 to 0.125
- exp_up: bfloat16 [8, 2048, 2048], P('ep', None, 'tp'), may hold values from -0.125 to 0.125
- exp_down: bfloat16 [8, 2048, 2048], P('ep', 'tp'), may hold values from -0.26516504 to 0.26516504
- sh_gate: bfloat16 [2048, 1024], P(None, 'tp'), may hold values from -0.125 to 0.125
- sh_up: bfloat16 [2048, 1024], P(None, 'tp'), may hold values from -0.125 to 0.125
- sh_down: bfloat16 [1024, 2048], P('tp'), may hold values from -0.375 to 0.375
- out_gain: bfloat16 [2048], P('tp'), may hold values from 0.099609375 to 1.8984375
Outputs:
- mixed: bfloat16 [512, 2048], P(('grp', 'ep'), 'tp'), parts along dimension 0
There are 2 independent parts, one for each index of `grp`. A program takes and returns all parts, laid end to end along the dimension named above; an argument that names none is the same for every part. Nothing has to cross between parts.
Inputs may be any that keep to these rules, and one draw needn't show every extreme that they name: `routes`: each row names 4 different experts; within the rows of one device (aligned blocks of 32 rows) no expert is named by more than 32 rows, a bound that some block reaches.
All inputs are finite; a program needn't handle non-finite values.
Results may differ from a plain program's by a relative error of at most 0.015.
Values may be sent and summed in bfloat16 or wider, within the bound.
No kernel may reach another device: no remote copies, remote signals or barrier semaphores. Data moves between devices by JAX's collectives and lax.ppermute only.
A program may use at most 64 MiB of HBM per device.

v0:
```python
import jax
import jax.numpy as jnp
from jax import lax
from jax.sharding import PartitionSpec as P

D = 2048


EPSILON = 1e-06


def slot_order(flat_routes, count):
    hits = (flat_routes[:, None] == jnp.arange(count, dtype=jnp.int32)[None, :]).astype(jnp.int32)
    before = jnp.cumsum(hits, axis=0) - hits
    return jnp.sum(before * hits, axis=1)


def slot_tables(position, flat_token, gate_values, slots_all):
    placed = position[:, None] == jnp.arange(slots_all, dtype=jnp.int32)[None, :]
    used = jnp.any(placed, axis=0)
    slot_token = jnp.sum(jnp.where(placed, flat_token[:, None], 0), axis=0)
    slot_gate = jnp.sum(jnp.where(placed, gate_values[:, None], jnp.float32(0.0)), axis=0)
    return (used, slot_token, slot_gate)


def shards(
    tokens, routes, gates, norm_gain, exp_gate, exp_up, exp_down, sh_gate, sh_up, sh_down, out_gain
):
    ep_count = lax.axis_size("ep")
    token_count, top_count = routes.shape
    local_count = exp_gate.shape[0]
    expert_count = local_count * ep_count
    capacity = min(
        token_count, max(2, 2 * ((token_count * top_count + expert_count - 1) // expert_count))
    )
    slots_all = ep_count * local_count * capacity
    values = tokens.astype(jnp.float32)
    normed = (
        values
        * lax.rsqrt(jnp.mean(values * values, axis=1, keepdims=True) + EPSILON)
        * norm_gain.astype(jnp.float32)
    ).astype(jnp.bfloat16)
    flat_expert = routes.reshape(-1)
    slot_index = slot_order(flat_expert, expert_count)
    flat_token = jnp.repeat(jnp.arange(token_count, dtype=jnp.int32), top_count)
    position = flat_expert * capacity + slot_index
    used, slot_token, slot_gate = slot_tables(position, flat_token, gates.reshape(-1), slots_all)
    send = jnp.where(used[:, None], normed[slot_token], jnp.zeros((), jnp.bfloat16))
    send = send.reshape(ep_count, local_count, capacity, normed.shape[1])
    received = lax.all_to_all(send, "ep", split_axis=0, concat_axis=0, tiled=True)
    gate_act = jnp.einsum("secd,edf->secf", received, exp_gate, preferred_element_type=jnp.float32)
    up_act = jnp.einsum("secd,edf->secf", received, exp_up, preferred_element_type=jnp.float32)
    hidden = (jax.nn.silu(gate_act) * up_act).astype(jnp.bfloat16)
    expert_part = jnp.einsum("secf,efd->secd", hidden, exp_down, preferred_element_type=jnp.float32)
    shared_gate = jnp.dot(normed, sh_gate, preferred_element_type=jnp.float32)
    shared_up = jnp.dot(normed, sh_up, preferred_element_type=jnp.float32)
    shared_hidden = (jax.nn.silu(shared_gate) * shared_up).astype(jnp.bfloat16)
    shared_part = jnp.dot(shared_hidden, sh_down, preferred_element_type=jnp.float32)
    expert_sum, shared_sum = (
        lax.psum_scatter(
            expert_part.astype(jnp.bfloat16), "tp", scatter_dimension=3, tiled=True
        ).astype(jnp.float32),
        lax.psum_scatter(
            shared_part.astype(jnp.bfloat16), "tp", scatter_dimension=1, tiled=True
        ).astype(jnp.float32),
    )
    expert_rows = expert_sum.astype(jnp.bfloat16)
    shared_values = lax.optimization_barrier(shared_sum.astype(jnp.bfloat16)).astype(jnp.float32)
    feature_count = expert_rows.shape[3]
    returned = lax.all_to_all(expert_rows, "ep", split_axis=0, concat_axis=0, tiled=True)
    pair_rows = returned.reshape(slots_all, feature_count)[position].astype(jnp.float32)
    routed = jnp.sum(
        gates[:, :, None] * pair_rows.reshape(token_count, top_count, feature_count), axis=1
    )
    total = routed + shared_values
    squares = jnp.sum(total * total, axis=1)
    whole_squares = lax.psum(squares, "tp")
    scale = lax.rsqrt(whole_squares / D + EPSILON)
    return (total * scale[:, None] * out_gain.astype(jnp.float32)).astype(jnp.bfloat16)


def solution(mesh):
    placed = (
        P(("grp", "ep"), None),
        P(("grp", "ep"), None),
        P(("grp", "ep"), None),
        P(),
        P("ep", None, "tp"),
        P("ep", None, "tp"),
        P("ep", "tp", None),
        P(None, "tp"),
        P(None, "tp"),
        P("tp", None),
        P("tp"),
    )
    return jax.shard_map(
        shards, mesh=mesh, in_specs=placed, out_specs=P(("grp", "ep"), "tp"), check_vma=False
    )
```

profile of v0, /device:TPU:0, one launch (start us, length us, event | category | flops | bytes accessed | tf_op | source)
XLA Modules:
  0.0 109.7 jit_solution(1442257461080784481)
XLA Ops:
  6.5 0.0 copy-start
  6.5 0.0 reduce-scatter.3.cloned.1.call-start
  6.5 1.2 %fusion.35 = f32[32]{0:T(128)S(1)} fusion(bf16[32,2048]{1,0:T(8,128)(2,1)} %param.11), kind=kLoop, calls=%fused_computation.25 | loop fusion | flops 196576 | bytes 131200 | tf_op jit(solution)/shard_map/reduce_sum | solution.py:40
  7.7 0.7 convert_element_type.55
  8.4 0.8 copy.24
  9.2 0.1 reshape.109
  9.3 0.1 broadcast_in_dim.45
  9.4 0.1 fusion.44
  9.5 0.2 reduce_window_sum.11
  9.7 0.2 select_reduce_fusion.1
  9.9 0.1 fusion.38
  10.0 0.1 select_reduce_fusion
  10.1 0.1 broadcast_in_dim.42
  10.2 1.0 fusion.37
  11.2 1.4 %gather_fusion = bf16[256,2048]{1,0:T(8,128)(2,1)S(1)} fusion(bf16[32,2048]{1,0:T(8,128)(2,1)S(1)} %fusion.37, s32[1024]{0:T(1024)S(1)} %pad_clamp_fusion.1), kind=kCustom, calls=%fused_computation | custom fusion | bytes 2098176 | tf_op jit(solution)/shard_map/gather | solution.py:48
  12.6 0.0 copy-start.5
  12.6 0.1 broadcast_select_fusion
  12.7 33.0 %all_to_all.10 = bf16[8,1,32,2048]{3,2,1,0:T(8,128)(2,1)S(1)} all-to-all(bf16[8,1,32,2048]{3,2,1,0:T(8,128)(2,1)S(1)} %broadcast_select_fusion), channel_id=1, replica_groups=mesh['grp'=2,'ep'=8,'tp'=2] {'ep'}, dimensions={0} | all-to-all | bytes 2097152 | tf_op jit(solution)/shard_map/all_to_all | solution.py:50
  45.7 0.0 copy-done.5
  45.7 2.3 %fusion.12 = f32[8,1,32,1024]{3,2,0,1:T(8,128)} fusion(bf16[1,2048,1024]{2,1,0:T(8,128)(2,1)S(1)} %copy-done.5, bf16[8,1,32,2048]{3,2,1,0:T(8,128)(2,1)S(1)} %all_to_all.10), kind=kOutput, calls=%fused_computation.11 | convolution fusion | flops 1073741824 | bytes 6291456 | tf_op jit(solution)/shard_map/secd,edf->secf/dot_general | solution.py:51
  48.0 7.2 %fusion.9 = bf16[8,1,32,2048]{3,2,0,1:T(8,128)(2,1)} fusion(bf16[1,1024,2048]{2,1,0:T(8,128)(2,1)} %param.17, bf16[1,2048,1024]{2,1,0:T(8,128)(2,1)} %param.16, bf16[8,1,32,2048]{3,2,1,0:T(8,128)(2,1)S(1)} %all_to_all.10, f32[8,1,32,1024]{3,2,0,1:T(8,128)} %fusion.12), kind=kOutput, calls=%fused_computation.9 | convolution fusion | flops 2149580800 | bytes 11534336 | tf_op jit(solution)/shard_map/secf,efd->secd/dot_general | solution.py:54
  55.3 0.0 reduce-scatter.3.cloned.1.call-update
  55.3 19.5 %reduce-scatter.3.cloned.1.call-done = bf16[8,1,32,1024]{3,2,0,1:T(8,128)(2,1)} async-done(((bf16[8,1,32,2048]{3,2,0,1:T(8,128)(2,1)}), bf16[8,1,32,1024]{3,2,0,1:T(8,128)(2,1)}) %reduce-scatter.3.cloned.1.call-update) | async-done | bytes 524304 | tf_op jit(solution)/shard_map/reduce_scatter | solution.py:60
  74.8 4.6 %all-to-all-start.1 = ((bf16[8,1,32,1024]{3,2,1,0:T(8,128)(2,1)}), bf16[8,1,32,1024]{3,2,1,0:T(8,128)(2,1)S(1)}, u32[]{:S(2)}, u32[]{:S(2)}) async-start(bf16[8,1,32,1024]{3,2,1,0:T(8,128)(2,1)} %bitcast.85), calls=%async_computation.2 | async-start | bytes 1048576 | tf_op jit(solution)/shard_map/all_to_all | solution.py:70
  79.4 0.0 reduce-scatter.5.cloned.1.call-start
  79.4 2.0 %fusion.49 = f32[32,512]{1,0:T(8,128)S(1)} fusion(bf16[32,2048]{1,0:T(8,128)(2,1)S(1)} %fusion.37, bf16[2048,512]{1,0:T(8,128)(2,1)} %param.18), kind=kOutput, calls=%fused_computation.55 | convolution fusion | flops 67108864 | bytes 2293760 | tf_op jit(solution)/shard_map/dot_general | solution.py:55
  81.5 0.0 copy-done
  81.5 0.0 copy-start.3
  81.5 0.0 copy-start.2
  81.5 0.0 copy-start.4
  81.5 3.2 %convolution_convert_fusion = bf16[32,2048]{1,0:T(8,128)(2,1)} fusion(bf16[512,2048]{1,0:T(8,128)(2,1)S(1)} %copy-done, bf16[32,2048]{1,0:T(8,128)(2,1)S(1)} %fusion.37, bf16[2048,512]{1,0:T(8,128)(2,1)} %param.19, f32[32,512]{1,0:T(8,128)S(1)} %fusion.49), kind=kOutput, calls=%fused_computation.10 | convolution fusion | flops 134381568 | bytes 4521984 | tf_op jit(solution)/shard_map/dot_general | solution.py:58
  84.7 0.0 reduce-scatter.5.cloned.1.call-update
  84.7 0.0 copy-done.3
  84.7 0.0 copy-done.2
  84.7 0.1 copy.27
  84.8 0.1 mul.99
  84.9 0.0 copy-done.4
  84.9 0.1 copy.23
  85.0 10.6 %reduce-scatter.5.cloned.1.call-done = bf16[32,1024]{1,0:T(8,128)(2,1)} async-done(((bf16[32,2048]{1,0:T(8,128)(2,1)}), bf16[32,1024]{1,0:T(8,128)(2,1)}) %reduce-scatter.5.cloned.1.call-update) | async-done | bytes 65552 | tf_op jit(solution)/shard_map/reduce_scatter | solution.py:63
  95.6 0.0 copy-start.1
  95.6 0.0 all-to-all-done.1
  95.6 0.9 gather_fusion.1
  96.5 0.2 reshape.116
  96.7 0.4 multiply_reduce_fusion
  97.1 0.0 copy-done.1
  97.1 0.1 multiply_reduce_fusion.1
  97.2 4.9 %psum.7 = f32[32]{0:T(128)S(1)} all-reduce(f32[32]{0:T(128)S(1)} %multiply_reduce_fusion.1), channel_id=1, replica_groups=mesh['grp'=2,'ep'=8,'tp'=2] {'tp'}, use_global_device_ids=true, to_apply=%region_9.10 | all-reduce | flops 32 | bytes 256 | tf_op jit(solution)/shard_map/psum | solution.py:77
  102.2 0.7 multiply_convert_fusion
  (10 shorter events, 0.1 us)
Async XLA Ops:
  6.5 74.9 %copy-start = (bf16[512,2048]{1,0:T(8,128)(2,1)S(1)}, bf16[512,2048]{1,0:T(8,128)(2,1)}, u32[]{:S(2)}) copy-start(bf16[512,2048]{1,0:T(8,128)(2,1)} %param.20) | copy-start | bytes 6291460
  6.5 68.2 %reduce-scatter.3.cloned.1.call-start = ((), (), s32[]{:S(2)}) async-start(), calls=%async_computation.4 | async-start | bytes 1572864 | tf_op jit(solution)/shard_map/reduce_scatter | solution.py:60
  12.6 33.1 %copy-start.5 = (bf16[1,2048,1024]{2,1,0:T(8,128)(2,1)S(1)}, bf16[1,2048,1024]{2,1,0:T(8,128)(2,1)}, u32[]{:S(2)}) copy-start(bf16[1,2048,1024]{2,1,0:T(8,128)(2,1)} %param.15) | copy-start | bytes 12582916
  74.8 20.9 %all-to-all-start.1 = ((bf16[8,1,32,1024]{3,2,1,0:T(8,128)(2,1)}), bf16[8,1,32,1024]{3,2,1,0:T(8,128)(2,1)S(1)}, u32[]{:S(2)}, u32[]{:S(2)}) async-start(bf16[8,1,32,1024]{3,2,1,0:T(8,128)(2,1)} %bitcast.85), calls=%async_computation.2 | async-start | bytes 1048576 | tf_op jit(solution)/shard_map/all_to_all | solution.py:70
  79.4 16.3 %reduce-scatter.5.cloned.1.call-start = ((), (), s32[]{:S(2)}) async-start(), calls=%async_computation.5 | async-start | bytes 196608 | tf_op jit(solution)/shard_map/reduce_scatter | solution.py:63
  81.5 3.2 %copy-start.3 = (bf16[1024]{0:T(1024)(128)(2,1)S(1)}, bf16[1024]{0:T(1024)(128)(2,1)}, u32[]{:S(2)}) copy-start(bf16[1024]{0:T(1024)(128)(2,1)} %param.21) | copy-start | bytes 6148
  81.5 3.2 %copy-start.2 = (s32[32,4]{0,1:T(4,128)S(1)}, s32[32,4]{0,1:T(4,128)}, u32[]{:S(2)}) copy-start(s32[32,4]{0,1:T(4,128)} %param.12) | copy-start | bytes 1540
  81.5 3.4 %copy-start.4 = (f32[32,4]{0,1:T(4,128)S(1)}, f32[32,4]{0,1:T(4,128)}, u32[]{:S(2)}) copy-start(f32[32,4]{0,1:T(4,128)} %param.13) | copy-start | bytes 1540
  95.6 1.4 %copy-start.1 = (bf16[32,1024]{1,0:T(8,128)(2,1)S(1)}, bf16[32,1024]{1,0:T(8,128)(2,1)}, u32[]{:S(2)}) copy-start(bf16[32,1024]{1,0:T(8,128)(2,1)} %reduce-scatter.5.cloned.1.call-done) | copy-start | bytes 196612
Sparse Core Ops, SparseCore 0:
  55.4 19.3 reduce-scatter.2
  84.8 10.8 reduce-scatter.4
where the time goes:
time: 110 us
  blocking collectives  37.9 us (34%)
  waiting for transfers between devices  30.1 us (27%)
  matrix products  14.7 us (13%)
  between operations  13.6 us (12%)
  other arithmetic  4.97 us (5%)
  starting transfers between devices  4.65 us (4%)
  local copies, waits for them, and re-layouts  3.77 us (3%)
    all_to_all x1, blocking collectives, shards(): lax.all_to_all(send, 'ep', split_axis=0, concat_axis=0, tiled=True)  33 us
    reduce_scatter x1, waiting for transfers between devices, shards(): lax.psum_scatter(expert_part.astype(jnp.bfloat16), 'tp', scatter_dimensio...  19.5 us
    reduce_scatter x1, waiting for transfers between devices, shards(): lax.psum_scatter(shared_part.astype(jnp.bfloat16), 'tp', scatter_dimensio...  10.6 us
    dot_general x1, matrix products, shards(): jnp.einsum('secf,efd->secd', hidden, exp_down, preferred_element_type=jnp...  7.21 us
    psum x1, blocking collectives, shards(): whole_squares = lax.psum(squares, 'tp')  4.93 us
    all_to_all x1, starting transfers between devices, shards(): lax.all_to_all(expert_rows, 'ep', split_axis=0, concat_axis=0, tiled=True)  4.61 us
    dot_general x1, matrix products, shards(): jnp.dot(shared_hidden, sh_down, preferred_element_type=jnp.float32)  3.15 us
    dot_general x1, matrix products, shards(): jnp.einsum('secd,edf->secf', received, exp_gate, preferred_element_type=j...  2.33 us
  transfers between devices with their start and end apart: 3, of which 2 were waited for; matrix products, arithmetic and copies ran while one was open for 5% of the time, Pallas kernels for 0%

commit v1 on v0

v1 whole, which is shorter than its diff:
```python
import jax
import jax.numpy as jnp
from jax import lax
from jax.sharding import PartitionSpec as P

EPSILON = 1e-06
LANES = 128


def shards(
    tokens, routes, gates, norm_gain, exp_gate, exp_up, exp_down, sh_gate, sh_up, sh_down, out_gain
):
    ep = lax.axis_size("ep")
    tp = lax.axis_size("tp")
    assert tp & (tp - 1) == 0 and ep & (ep - 1) == 0 and exp_gate.shape[0] == 1
    rows, width = tokens.shape
    half = width // tp
    chips = ep // 2
    me = lax.axis_index("ep")
    side = lax.axis_index("tp")
    f32, bf16 = jnp.float32, jnp.bfloat16

    def across(x, bits):
        return lax.ppermute(x, "ep", [(i, i ^ bits) for i in range(ep)])

    def over_tp(x, bits):
        return lax.ppermute(x, "tp", [(i, i ^ bits) for i in range(tp)])

    def features(x, index):
        if tp == 2:
            return jnp.where(index == 0, x[..., :half], x[..., half:])
        return lax.dynamic_slice_in_dim(x, index * half, half, axis=x.ndim - 1)

    values = tokens.astype(f32)
    normed = (
        values
        * lax.rsqrt(jnp.mean(values * values, axis=1, keepdims=True) + EPSILON)
        * norm_gain.astype(f32)
    ).astype(bf16)
    extra = (2 * ep + LANES - 1) // LANES * LANES
    column = jnp.arange(extra, dtype=jnp.int32)
    weight = jnp.sum(
        jnp.where(routes[:, :, None] == (column % ep)[None, None, :], gates[:, :, None], 0.0), axis=1
    )
    coarse = weight.astype(bf16)
    fine = (weight - coarse.astype(f32)).astype(bf16)
    packed = jnp.where(column < ep, coarse, jnp.where(column < 2 * ep, fine, jnp.zeros((), bf16)))
    block = jnp.concatenate([normed, packed], axis=1)

    mine = [block] + [across(block, 2 * k) for k in range(1, chips)]
    theirs = [across(b, 1) for b in mine]

    shared_gate = jnp.dot(normed, sh_gate, preferred_element_type=f32)
    shared_up = jnp.dot(normed, sh_up, preferred_element_type=f32)
    shared_hidden = (jax.nn.silu(shared_gate) * shared_up).astype(bf16)
    shared_part = jnp.dot(shared_hidden, sh_down, preferred_element_type=f32)

    gathered = jnp.concatenate(theirs + mine, axis=0)
    inputs = gathered[:, :width]
    lanes = gathered[:, width:].astype(f32)
    mix = jnp.sum(jnp.where((column % ep == me)[None, :] & (column < 2 * ep), lanes, 0.0), axis=1)
    gate_act = jnp.dot(inputs, exp_gate[0], preferred_element_type=f32)
    up_act = jnp.dot(inputs, exp_up[0], preferred_element_type=f32)
    hidden = (jax.nn.silu(gate_act) * up_act * mix[:, None]).astype(bf16)
    part = jnp.dot(hidden, exp_down[0], preferred_element_type=f32).astype(bf16)

    other = across(part[: chips * rows], 1)
    paired = part[chips * rows :].astype(f32) + other.astype(f32)
    paired = paired.reshape(chips, rows, width)
    paired = [paired[0] + shared_part] + [paired[k] for k in range(1, chips)]
    arrived = {}
    for k in list(range(1, chips)) + [0]:
        arrived[k] = features(paired[k], side)
        for bits in range(1, tp):
            sent = features(paired[k], side ^ bits).astype(bf16)
            arrived[k] = arrived[k] + over_tp(sent, bits).astype(f32)
    total = arrived[0]
    for k in range(1, chips):
        total = total + across(arrived[k].astype(bf16), 2 * k).astype(f32)
    own_squares = jnp.sum(total * total, axis=1)
    squares = own_squares
    for bits in range(1, tp):
        squares = squares + over_tp(own_squares, bits)
    scale = lax.rsqrt(squares / width + EPSILON)
    return (total * scale[:, None] * out_gain.astype(f32)).astype(bf16)


def solution(mesh):
    placed = (
        P(("grp", "ep"), None),
        P(("grp", "ep"), None),
        P(("grp", "ep"), None),
        P(),
        P("ep", None, "tp"),
        P("ep", None, "tp"),
        P("ep", "tp", None),
        P(None, "tp"),
        P(None, "tp"),
        P("tp", None),
        P("tp"),
    )
    return jax.shard_map(
        shards, mesh=mesh, in_specs=placed, out_specs=P(("grp", "ep"), "tp"), check_vma=False
    )
```

time: 110 us -> 63.6 us (0.58)
  blocking collectives: 37.9 us -> 0 us
  between operations: 13.6 us -> 0.14 us
  starting transfers between devices: 4.65 us -> 17.7 us
  waiting for transfers between devices: 30.1 us -> 19.6 us
  other arithmetic: 4.97 us -> 7.73 us
  local copies, waits for them, and re-layouts: 3.77 us -> 1.9 us
  matrix products: 14.7 us -> 16.2 us
    all_to_all x1 -> x0, blocking collectives: 33 us -> none  [shards(): lax.all_to_all(send, 'ep', split_axis=0, concat_axis=0, tiled=True)]
    reduce_scatter x2 -> x0, waiting for transfers between devices: 30.1 us -> none  [the longest x1 19.5 us: shards(): lax.psum_scatter(expert_part.astype(jnp.bfloat16), 'tp', scatter_dimensio...]
    ppermute x0 -> x16, waiting for transfers between devices: none -> 19.6 us  [the longest x11 16.8 us: across(): return lax.ppermute(x, 'ep', [(i, i ^ bits) for i in range(ep)])]
    ppermute x0 -> x16, starting transfers between devices: none -> 17.7 us  [the longest x11 12 us: across(): return lax.ppermute(x, 'ep', [(i, i ^ bits) for i in range(ep)])]
    psum x1 -> x0, blocking collectives: 4.93 us -> none  [shards(): whole_squares = lax.psum(squares, 'tp')]
    all_to_all x1 -> x0, starting transfers between devices: 4.61 us -> none  [shards(): lax.all_to_all(expert_rows, 'ep', split_axis=0, concat_axis=0, tiled=True)]
    gather x2 -> x0, local copies, waits for them, and re-layouts: 2.22 us -> none  [the longest x1 1.36 us: shards(): normed[slot_token]]
    convert_element_type x4 -> x6, other arithmetic: 1.51 us -> 3.22 us  [the longest x1 0.96 us: shards(): total = total + across(arrived[k].astype(bf16), 2 * k).astype(f32)]
  transfers between devices with their start and end apart: 3 -> 16, of which waited for: 2 -> 7; matrix products, arithmetic and copies ran while one was open for 5% -> 10% of each run, Pallas kernels for 0% -> 0%
where the time goes in v1:
time: 63.6 us; the launch traced here: 63.2 us
  waiting for transfers between devices  19.6 us (31%)
  starting transfers between devices  17.7 us (28%)
  matrix products  16.2 us (25%)
  other arithmetic  7.73 us (12%)
  local copies, waits for them, and re-layouts  1.9 us (3%)
    ppermute x11, waiting for transfers between devices, across(): return lax.ppermute(x, 'ep', [(i, i ^ bits) for i in range(ep)])  16.8 us
    ppermute x11, starting transfers between devices, across(): return lax.ppermute(x, 'ep', [(i, i ^ bits) for i in range(ep)])  12 us
    dot_general x1, matrix products, shards(): part = jnp.dot(hidden, exp_down[0], preferred_element_type=f32).astype(bf16)  6.52 us
    ppermute x5, starting transfers between devices, over_tp(): return lax.ppermute(x, 'tp', [(i, i ^ bits) for i in range(tp)])  5.73 us
    dot_general x1, matrix products, shards(): gate_act = jnp.dot(inputs, exp_gate[0], preferred_element_type=f32)  4.48 us
    ppermute x5, waiting for transfers between devices, over_tp(): return lax.ppermute(x, 'tp', [(i, i ^ bits) for i in range(tp)])  2.75 us
    dot_general x1, matrix products, shards(): shared_gate = jnp.dot(normed, sh_gate, preferred_element_type=f32)  2.68 us
    dot_general x1, matrix products, shards(): shared_part = jnp.dot(shared_hidden, sh_down, preferred_element_type=f32)  2.49 us
  transfers between devices with their start and end apart: 16, of which 7 were waited for; matrix products, arithmetic and copies ran while one was open for 10% of the time, Pallas kernels for 0%

profile of v1, /device:TPU:0, one launch (start us, length us, event | category | flops | bytes accessed | tf_op | source)
XLA Modules:
  0.0 63.2 jit_solution(10337623770887580853)
XLA Ops:
  0.0 0.8 %convert_element_type.85 = f32[2048]{0:T(1024)S(1)} convert(bf16[2048]{0:T(1024)(128)(2,1)} %param.14) | non-fusion elementwise | flops 2048 | bytes 12288 | tf_op jit(solution)/shard_map/convert_element_type | solution.py:38
  0.9 1.0 %fusion.23 = f32[32]{0:T(128)S(1)} fusion(bf16[32,2048]{1,0:T(8,128)(2,1)} %param.11), kind=kLoop, calls=%fused_computation.18 | loop fusion | flops 196576 | bytes 131200 | tf_op jit(solution)/shard_map/reduce_sum | solution.py:37
  1.9 1.0 %fusion.25 = bf16[32,2048]{1,0:T(8,128)(2,1)S(1)} fusion(bf16[32,2048]{1,0:T(8,128)(2,1)} %param.11, f32[2048]{0:T(1024)S(1)} %convert_element_type.85, f32[32]{0:T(128)S(1)} %add_rsqrt_fusion.1), kind=kLoop, calls=%fused_computation.20 | loop fusion | flops 262144 | bytes 270464 | tf_op jit(solution)/shard_map/convert_element_type | solution.py:39
  2.9 0.8 %select_reduce_fusion.1 = f32[32,128]{1,0:T(8,128)S(1)} fusion(f32[32,4]{0,1:T(4,128)} %param.13, s32[128]{0:T(128)S(1)} %and_select_fusion, s32[32,4]{0,1:T(4,128)} %param.12), kind=kLoop, calls=%fused_computation.39 | loop fusion | flops 45056 | bytes 17920 | tf_op jit(solution)/shard_map/reduce_sum | solution.py:42
  3.8 3.1 %collective-permute-start.1 = (bf16[32,2176]{1,0:T(8,128)(2,1)S(1)}, bf16[32,2176]{1,0:T(8,128)(2,1)S(1)}, u32[]{:S(2)}, u32[]{:S(2)}) collective-permute-start(bf16[32,2176]{1,0:T(8,128)(2,1)S(1)} %pad_maximum_fusion), channel_id=1, source_target_pairs={{0,4},{2,6},{4,0},{6,2},{8,12},{10,14},{12,8},{14,10},{1,5},{3,7},... | collective-permute-start | bytes 417800 | tf_op jit(solution)/shard_map/ppermute | solution.py:24
  6.9 0.0 collective-permute-start
  6.9 2.6 %collective-permute-start.3 = (bf16[32,2176]{1,0:T(8,128)(2,1)S(1)}, bf16[32,2176]{1,0:T(8,128)(2,1)S(1)}, u32[]{:S(2)}, u32[]{:S(2)}) collective-permute-start(bf16[32,2176]{1,0:T(8,128)(2,1)S(1)} %pad_maximum_fusion), channel_id=1, source_target_pairs={{0,8},{2,10},{4,12},{6,14},{8,0},{10,2},{12,4},{14,6},{1,9},{3,11}... | collective-permute-start | bytes 417800 | tf_op jit(solution)/shard_map/ppermute | solution.py:24
  9.5 0.0 collective-permute-start.5
  9.5 1.1 %collective-permute-done.1 = bf16[32,2176]{1,0:T(8,128)(2,1)S(1)} collective-permute-done((bf16[32,2176]{1,0:T(8,128)(2,1)S(1)}, bf16[32,2176]{1,0:T(8,128)(2,1)S(1)}, u32[]{:S(2)}, u32[]{:S(2)}) %collective-permute-start.1) | collective-permute-done | bytes 139296 | tf_op jit(solution)/shard_map/ppermute | solution.py:24
  10.5 0.0 collective-permute-start.2
  10.6 0.0 collective-permute-done
  10.6 9.7 %collective-permute-done.3 = bf16[32,2176]{1,0:T(8,128)(2,1)S(1)} collective-permute-done((bf16[32,2176]{1,0:T(8,128)(2,1)S(1)}, bf16[32,2176]{1,0:T(8,128)(2,1)S(1)}, u32[]{:S(2)}, u32[]{:S(2)}) %collective-permute-start.3) | collective-permute-done | bytes 139296 | tf_op jit(solution)/shard_map/ppermute | solution.py:24
  20.3 0.0 collective-permute-start.4
  20.3 0.0 collective-permute-done.5
  20.3 0.5 collective-permute-start.6
  20.8 0.0 collective-permute-done.2
  20.8 0.8 %collective-permute-done.4 = bf16[32,2176]{1,0:T(8,128)(2,1)S(1)} collective-permute-done((bf16[32,2176]{1,0:T(8,128)(2,1)S(1)}, bf16[32,2176]{1,0:T(8,128)(2,1)S(1)}, u32[]{:S(2)}, u32[]{:S(2)}) %collective-permute-start.4) | collective-permute-done | bytes 139296 | tf_op jit(solution)/shard_map/ppermute | solution.py:24
  21.7 0.2 collective-permute-done.6
  22.0 0.1 select_reduce_fusion
  22.1 0.9 %copy-done.2 = bf16[256,2176]{1,0:T(8,128)(2,1)} copy-done((bf16[256,2176]{1,0:T(8,128)(2,1)}, bf16[256,2176]{1,0:T(8,128)(2,1)S(1)}, u32[]{:S(2)}) %copy-start.2) | copy-done | bytes 1114136
  23.0 4.5 %fusion.4 = f32[256,1024]{1,0:T(8,128)} fusion(bf16[1,2048,1024]{2,1,0:T(8,128)(2,1)} %param.15, bf16[256,2176]{1,0:T(8,128)(2,1)S(1)} %constant_dynamic-update-slice_fusion), kind=kOutput, calls=%fused_computation.4 | convolution fusion | flops 1073741824 | bytes 6291456 | tf_op jit(solution)/shard_map/dot_general | solution.py:62
  27.4 6.5 %fusion.6 = bf16[256,2048]{1,0:T(8,128)(2,1)S(1)} fusion(bf16[1,1024,2048]{2,1,0:T(8,128)(2,1)} %param.17, f32[256,1024]{1,0:T(8,128)} %fusion.4, bf16[1,2048,1024]{2,1,0:T(8,128)(2,1)} %param.16, bf16[256,2176]{1,0:T(8,128)(2,1)} %copy-done.2, f32[256]{0:T(256)S(1)} %select_reduce_fusion), kind=kOutput, calls=%fused_computation.6 | convolution fusion | flops 2149842944 | bytes 11535360 | tf_op jit(solution)/shard_map/dot_general | solution.py:65
  34.0 0.9 %slice.76 = bf16[128,2048]{1,0:T(8,128)(2,1)} slice(bf16[256,2048]{1,0:T(8,128)(2,1)S(1)} %fusion.6), slice={[0:128], [0:2048]} | slice | bytes 1048576 | tf_op jit(solution)/shard_map/slice | solution.py:67
  34.9 0.3 collective-permute-start.7
  35.2 2.7 %fusion.36 = f32[32,512]{1,0:T(8,128)} fusion(bf16[32,2048]{1,0:T(8,128)(2,1)S(1)} %fusion.25, bf16[2048,512]{1,0:T(8,128)(2,1)} %param.18), kind=kOutput, calls=%fused_computation.60 | convolution fusion | flops 67108864 | bytes 2293760 | tf_op jit(solution)/shard_map/dot_general | solution.py:53
  37.9 0.0 collective-permute-done.7
  37.9 1.3 %convert_add_fusion = f32[128,2048]{1,0:T(8,128)S(1)} fusion(bf16[128,2048]{1,0:T(8,128)(2,1)} %collective-permute-done.7, bf16[256,2048]{1,0:T(8,128)(2,1)} %copy-done.1), kind=kLoop, calls=%fused_computation.10 | loop fusion | flops 786432 | bytes 2097152 | tf_op jit(solution)/shard_map/add | solution.py:68
  39.2 0.7 %select_convert_fusion.2 = (bf16[32,1024]{1,0:T(8,128)(2,1)}, bf16[32,1024]{1,0:T(8,128)(2,1)}, bf16[32,1024]{1,0:T(8,128)(2,1)}) fusion(f32[128,2048]{1,0:T(8,128)S(1)} %convert_add_fusion, pred[]{:T(512)S(6)} %eq.44), kind=kLoop, calls=%fused_computation.31 | loop fusion | flops 98304 | bytes 589825 | tf_op jit(solution)/shard_map/convert_element_type | solution.py:75
  39.9 1.5 %collective-permute-start.11 = (bf16[32,1024]{1,0:T(8,128)(2,1)}, bf16[32,1024]{1,0:T(8,128)(2,1)}, u32[]{:S(2)}, u32[]{:S(2)}) collective-permute-start(bf16[32,1024]{1,0:T(8,128)(2,1)} %get-tuple-element.12), channel_id=1, source_target_pairs={{0,1},{1,0},{2,3},{3,2},{4,5},{5,4},{6,7},{7,6},{8,9},{9,8},{10,11... | collective-permute-start | bytes 196616 | tf_op jit(solution)/shard_map/ppermute | solution.py:27
  41.4 0.5 collective-permute-start.13
  41.9 1.5 %collective-permute-start.9 = (bf16[32,1024]{1,0:T(8,128)(2,1)}, bf16[32,1024]{1,0:T(8,128)(2,1)}, u32[]{:S(2)}, u32[]{:S(2)}) collective-permute-start(bf16[32,1024]{1,0:T(8,128)(2,1)} %get-tuple-element.10), channel_id=1, source_target_pairs={{0,1},{1,0},{2,3},{3,2},{4,5},{5,4},{6,7},{7,6},{8,9},{9,8},{10,11... | collective-permute-start | bytes 196616 | tf_op jit(solution)/shard_map/ppermute | solution.py:27
  43.4 2.5 %slice_add_fusion = f32[32,2048]{1,0:T(8,128)S(1)} fusion(f32[128,2048]{1,0:T(8,128)S(1)} %convert_add_fusion, bf16[512,2048]{1,0:T(8,128)(2,1)S(1)} %copy-done, bf16[32,2048]{1,0:T(8,128)(2,1)S(1)} %fusion.25, bf16[2048,512]{1,0:T(8,128)(2,1)} %param.19, f32[32,512]{1,0:T(8,128)} %fusion.36), kind=kOutput, calls=%fused_computation.21 | convolution fusion | flops 134381568 | bytes 4915200 | tf_op jit(solution)/shard_map/dot_general | solution.py:56
  45.9 0.0 copy-start.3
  45.9 0.6 collective-permute-start.8
  46.5 0.0 collective-permute-done.11
  46.5 0.0 collective-permute-done.13
  46.6 0.7 %collective-permute-done.9 = bf16[32,1024]{1,0:T(8,128)(2,1)} collective-permute-done((bf16[32,1024]{1,0:T(8,128)(2,1)}, bf16[32,1024]{1,0:T(8,128)(2,1)}, u32[]{:S(2)}, u32[]{:S(2)}) %collective-permute-start.9) | collective-permute-done | bytes 65568 | tf_op jit(solution)/shard_map/ppermute | solution.py:27
  47.3 1.0 %add_convert_fusion.2 = (bf16[32,1024]{1,0:T(8,128)(2,1)S(1)}, bf16[32,1024]{1,0:T(8,128)(2,1)S(1)}, bf16[32,1024]{1,0:T(8,128)(2,1)S(1)}) fusion(bf16[32,1024]{1,0:T(8,128)(2,1)} %collective-permute-done.9, f32[128,2048]{1,0:T(8,128)S(1)} %convert_add_fusion, pred[]{:T(512)S(6)} %eq.38, bf16[32,1024]{1,0:T(8,128)(2,1)} %collective-permute-done.13, ...), kind=kLoop, calls=%fused_computation.30 | loop fusion | flops 393216 | bytes 1179649 | tf_op jit(solution)/shard_map/convert_element_type | solution.py:79
  48.2 2.9 %collective-permute-start.10 = (bf16[32,1024]{1,0:T(8,128)(2,1)S(1)}, bf16[32,1024]{1,0:T(8,128)(2,1)S(1)}, u32[]{:S(2)}, u32[]{:S(2)}) collective-permute-start(bf16[32,1024]{1,0:T(8,128)(2,1)S(1)} %get-tuple-element.7), channel_id=1, source_target_pairs={{0,4},{2,6},{4,0},{6,2},{8,12},{10,14},{12,8},{14,10},{1,5},{3,7},... | collective-permute-start | bytes 196616 | tf_op jit(solution)/shard_map/ppermute | solution.py:24
  51.1 1.1 %collective-permute-start.12 = (bf16[32,1024]{1,0:T(8,128)(2,1)S(1)}, bf16[32,1024]{1,0:T(8,128)(2,1)S(1)}, u32[]{:S(2)}, u32[]{:S(2)}) collective-permute-start(bf16[32,1024]{1,0:T(8,128)(2,1)S(1)} %get-tuple-element.9), channel_id=1, source_target_pairs={{0,8},{2,10},{4,12},{6,14},{8,0},{10,2},{12,4},{14,6},{1,9},{3,11}... | collective-permute-start | bytes 196616 | tf_op jit(solution)/shard_map/ppermute | solution.py:24
  52.3 1.4 %collective-permute-start.14 = (bf16[32,1024]{1,0:T(8,128)(2,1)S(1)}, bf16[32,1024]{1,0:T(8,128)(2,1)S(1)}, u32[]{:S(2)}, u32[]{:S(2)}) collective-permute-start(bf16[32,1024]{1,0:T(8,128)(2,1)S(1)} %get-tuple-element.8), channel_id=1, source_target_pairs={{0,12},{2,14},{4,8},{6,10},{8,4},{10,6},{12,0},{14,2},{1,13},{3,15... | collective-permute-start | bytes 196616 | tf_op jit(solution)/shard_map/ppermute | solution.py:24
  53.6 0.0 collective-permute-done.8
  53.6 0.0 collective-permute-done.10
  53.6 5.0 %collective-permute-done.12 = bf16[32,1024]{1,0:T(8,128)(2,1)S(1)} collective-permute-done((bf16[32,1024]{1,0:T(8,128)(2,1)S(1)}, bf16[32,1024]{1,0:T(8,128)(2,1)S(1)}, u32[]{:S(2)}, u32[]{:S(2)}) %collective-permute-start.12) | collective-permute-done | bytes 65568 | tf_op jit(solution)/shard_map/ppermute | solution.py:24
  58.7 0.2 multiply_reduce_fusion
  58.9 1.6 %collective-permute-start.15 = (f32[32]{0:T(128)S(1)}, f32[32]{0:T(128)S(1)}, u32[]{:S(2)}, u32[]{:S(2)}) collective-permute-start(f32[32]{0:T(128)S(1)} %get-tuple-element.5), channel_id=1, source_target_pairs={{0,1},{1,0},{2,3},{3,2},{4,5},{5,4},{6,7},{7,6},{8,9},{9,8},{10,11... | collective-permute-start | bytes 392 | tf_op jit(solution)/shard_map/ppermute | solution.py:27
  60.5 2.0 %collective-permute-done.15 = f32[32]{0:T(128)S(1)} collective-permute-done((f32[32]{0:T(128)S(1)}, f32[32]{0:T(128)S(1)}, u32[]{:S(2)}, u32[]{:S(2)}) %collective-permute-start.15) | collective-permute-done | bytes 160 | tf_op jit(solution)/shard_map/ppermute | solution.py:27
  62.5 0.7 %multiply_convert_fusion.1 = bf16[32,1024]{1,0:T(8,128)(2,1)} fusion(f32[32,1024]{1,0:T(8,128)S(1)} %get-tuple-element.6, f32[1024]{0:T(1024)S(1)} %convert_element_type.110, f32[32]{0:T(128)S(1)} %add_rsqrt_fusion), kind=kLoop, calls=%fused_computation.23 | loop fusion | flops 98304 | bytes 200832 | tf_op jit(solution)/shard_map/convert_element_type | solution.py:85
  (24 shorter events, 0.2 us)
Async XLA Ops:
  0.0 43.4 %copy-start = (bf16[512,2048]{1,0:T(8,128)(2,1)S(1)}, bf16[512,2048]{1,0:T(8,128)(2,1)}, u32[]{:S(2)}) copy-start(bf16[512,2048]{1,0:T(8,128)(2,1)} %param.20) | copy-start | bytes 6291460
  3.8 6.8 %collective-permute-start.1 = (bf16[32,2176]{1,0:T(8,128)(2,1)S(1)}, bf16[32,2176]{1,0:T(8,128)(2,1)S(1)}, u32[]{:S(2)}, u32[]{:S(2)}) collective-permute-start(bf16[32,2176]{1,0:T(8,128)(2,1)S(1)} %pad_maximum_fusion), channel_id=1, source_target_pairs={{0,4},{2,6},{4,0},{6,2},{8,12},{10,14},{12,8},{14,10},{1,5},{3,7},... | collective-permute-start | bytes 417800 | tf_op jit(solution)/shard_map/ppermute | solution.py:24
  6.9 3.7 %collective-permute-start = (bf16[32,2176]{1,0:T(8,128)(2,1)S(1)}, bf16[32,2176]{1,0:T(8,128)(2,1)S(1)}, u32[]{:S(2)}, u32[]{:S(2)}) collective-permute-start(bf16[32,2176]{1,0:T(8,128)(2,1)S(1)} %pad_maximum_fusion), channel_id=1, source_target_pairs={{0,2},{2,0},{4,6},{6,4},{8,10},{10,8},{12,14},{14,12},{1,3},{3,1},... | collective-permute-start | bytes 417800 | tf_op jit(solution)/shard_map/ppermute | solution.py:24
  6.9 13.4 %collective-permute-start.3 = (bf16[32,2176]{1,0:T(8,128)(2,1)S(1)}, bf16[32,2176]{1,0:T(8,128)(2,1)S(1)}, u32[]{:S(2)}, u32[]{:S(2)}) collective-permute-start(bf16[32,2176]{1,0:T(8,128)(2,1)S(1)} %pad_maximum_fusion), channel_id=1, source_target_pairs={{0,8},{2,10},{4,12},{6,14},{8,0},{10,2},{12,4},{14,6},{1,9},{3,11}... | collective-permute-start | bytes 417800 | tf_op jit(solution)/shard_map/ppermute | solution.py:24
  9.5 10.8 %collective-permute-start.5 = (bf16[32,2176]{1,0:T(8,128)(2,1)S(1)}, bf16[32,2176]{1,0:T(8,128)(2,1)S(1)}, u32[]{:S(2)}, u32[]{:S(2)}) collective-permute-start(bf16[32,2176]{1,0:T(8,128)(2,1)S(1)} %pad_maximum_fusion), channel_id=1, source_target_pairs={{0,12},{2,14},{4,8},{6,10},{8,4},{10,6},{12,0},{14,2},{1,13},{3,15... | collective-permute-start | bytes 417800 | tf_op jit(solution)/shard_map/ppermute | solution.py:24
  10.5 10.3 %collective-permute-start.2 = (bf16[32,2176]{1,0:T(8,128)(2,1)S(1)}, bf16[32,2176]{1,0:T(8,128)(2,1)S(1)}, u32[]{:S(2)}, u32[]{:S(2)}) collective-permute-start(bf16[32,2176]{1,0:T(8,128)(2,1)S(1)} %collective-permute-done.1), channel_id=1, source_target_pairs={{0,2},{2,0},{4,6},{6,4},{8,10},{10,8},{12,14},{14,12},{1,3},{3,1},... | collective-permute-start | bytes 417800 | tf_op jit(solution)/shard_map/ppermute | solution.py:24
  20.3 1.4 %collective-permute-start.4 = (bf16[32,2176]{1,0:T(8,128)(2,1)S(1)}, bf16[32,2176]{1,0:T(8,128)(2,1)S(1)}, u32[]{:S(2)}, u32[]{:S(2)}) collective-permute-start(bf16[32,2176]{1,0:T(8,128)(2,1)S(1)} %collective-permute-done.3), channel_id=1, source_target_pairs={{0,2},{2,0},{4,6},{6,4},{8,10},{10,8},{12,14},{14,12},{1,3},{3,1},... | collective-permute-start | bytes 417800 | tf_op jit(solution)/shard_map/ppermute | solution.py:24
  20.3 1.6 %collective-permute-start.6 = (bf16[32,2176]{1,0:T(8,128)(2,1)S(1)}, bf16[32,2176]{1,0:T(8,128)(2,1)S(1)}, u32[]{:S(2)}, u32[]{:S(2)}) collective-permute-start(bf16[32,2176]{1,0:T(8,128)(2,1)S(1)} %collective-permute-done.5), channel_id=1, source_target_pairs={{0,2},{2,0},{4,6},{6,4},{8,10},{10,8},{12,14},{14,12},{1,3},{3,1},... | collective-permute-start | bytes 417800 | tf_op jit(solution)/shard_map/ppermute | solution.py:24
  22.0 1.0 %copy-start.2 = (bf16[256,2176]{1,0:T(8,128)(2,1)}, bf16[256,2176]{1,0:T(8,128)(2,1)S(1)}, u32[]{:S(2)}) copy-start(bf16[256,2176]{1,0:T(8,128)(2,1)S(1)} %constant_dynamic-update-slice_fusion) | copy-start | bytes 3342340
  34.0 3.9 %copy-start.1 = (bf16[256,2048]{1,0:T(8,128)(2,1)}, bf16[256,2048]{1,0:T(8,128)(2,1)S(1)}, u32[]{:S(2)}) copy-start(bf16[256,2048]{1,0:T(8,128)(2,1)S(1)} %fusion.6) | copy-start | bytes 3145732
  34.9 3.0 %collective-permute-start.7 = (bf16[128,2048]{1,0:T(8,128)(2,1)}, bf16[128,2048]{1,0:T(8,128)(2,1)}, u32[]{:S(2)}, u32[]{:S(2)}) collective-permute-start(bf16[128,2048]{1,0:T(8,128)(2,1)} %slice.76), channel_id=1, source_target_pairs={{0,2},{2,0},{4,6},{6,4},{8,10},{10,8},{12,14},{14,12},{1,3},{3,1},... | collective-permute-start | bytes 1572872 | tf_op jit(solution)/shard_map/ppermute | solution.py:24
  39.9 6.7 %collective-permute-start.11 = (bf16[32,1024]{1,0:T(8,128)(2,1)}, bf16[32,1024]{1,0:T(8,128)(2,1)}, u32[]{:S(2)}, u32[]{:S(2)}) collective-permute-start(bf16[32,1024]{1,0:T(8,128)(2,1)} %get-tuple-element.12), channel_id=1, source_target_pairs={{0,1},{1,0},{2,3},{3,2},{4,5},{5,4},{6,7},{7,6},{8,9},{9,8},{10,11... | collective-permute-start | bytes 196616 | tf_op jit(solution)/shard_map/ppermute | solution.py:27
  41.4 5.2 %collective-permute-start.13 = (bf16[32,1024]{1,0:T(8,128)(2,1)}, bf16[32,1024]{1,0:T(8,128)(2,1)}, u32[]{:S(2)}, u32[]{:S(2)}) collective-permute-start(bf16[32,1024]{1,0:T(8,128)(2,1)} %get-tuple-element.11), channel_id=1, source_target_pairs={{0,1},{1,0},{2,3},{3,2},{4,5},{5,4},{6,7},{7,6},{8,9},{9,8},{10,11... | collective-permute-start | bytes 196616 | tf_op jit(solution)/shard_map/ppermute | solution.py:27
  41.9 5.4 %collective-permute-start.9 = (bf16[32,1024]{1,0:T(8,128)(2,1)}, bf16[32,1024]{1,0:T(8,128)(2,1)}, u32[]{:S(2)}, u32[]{:S(2)}) collective-permute-start(bf16[32,1024]{1,0:T(8,128)(2,1)} %get-tuple-element.10), channel_id=1, source_target_pairs={{0,1},{1,0},{2,3},{3,2},{4,5},{5,4},{6,7},{7,6},{8,9},{9,8},{10,11... | collective-permute-start | bytes 196616 | tf_op jit(solution)/shard_map/ppermute | solution.py:27
  45.9 14.6 %copy-start.3 = (bf16[1024]{0:T(1024)(128)(2,1)S(1)}, bf16[1024]{0:T(1024)(128)(2,1)}, u32[]{:S(2)}) copy-start(bf16[1024]{0:T(1024)(128)(2,1)} %param.21) | copy-start | bytes 6148
  45.9 7.7 %collective-permute-start.8 = (bf16[32,1024]{1,0:T(8,128)(2,1)S(1)}, bf16[32,1024]{1,0:T(8,128)(2,1)S(1)}, u32[]{:S(2)}, u32[]{:S(2)}) collective-permute-start(bf16[32,1024]{1,0:T(8,128)(2,1)S(1)} %select_convert_fusion.3), channel_id=1, source_target_pairs={{0,1},{1,0},{2,3},{3,2},{4,5},{5,4},{6,7},{7,6},{8,9},{9,8},{10,11... | collective-permute-start | bytes 196616 | tf_op jit(solution)/shard_map/ppermute | solution.py:27
  48.2 5.4 %collective-permute-start.10 = (bf16[32,1024]{1,0:T(8,128)(2,1)S(1)}, bf16[32,1024]{1,0:T(8,128)(2,1)S(1)}, u32[]{:S(2)}, u32[]{:S(2)}) collective-permute-start(bf16[32,1024]{1,0:T(8,128)(2,1)S(1)} %get-tuple-element.7), channel_id=1, source_target_pairs={{0,4},{2,6},{4,0},{6,2},{8,12},{10,14},{12,8},{14,10},{1,5},{3,7},... | collective-permute-start | bytes 196616 | tf_op jit(solution)/shard_map/ppermute | solution.py:24
  51.1 7.6 %collective-permute-start.12 = (bf16[32,1024]{1,0:T(8,128)(2,1)S(1)}, bf16[32,1024]{1,0:T(8,128)(2,1)S(1)}, u32[]{:S(2)}, u32[]{:S(2)}) collective-permute-start(bf16[32,1024]{1,0:T(8,128)(2,1)S(1)} %get-tuple-element.9), channel_id=1, source_target_pairs={{0,8},{2,10},{4,12},{6,14},{8,0},{10,2},{12,4},{14,6},{1,9},{3,11}... | collective-permute-start | bytes 196616 | tf_op jit(solution)/shard_map/ppermute | solution.py:24
  52.3 6.4 %collective-permute-start.14 = (bf16[32,1024]{1,0:T(8,128)(2,1)S(1)}, bf16[32,1024]{1,0:T(8,128)(2,1)S(1)}, u32[]{:S(2)}, u32[]{:S(2)}) collective-permute-start(bf16[32,1024]{1,0:T(8,128)(2,1)S(1)} %get-tuple-element.8), channel_id=1, source_target_pairs={{0,12},{2,14},{4,8},{6,10},{8,4},{10,6},{12,0},{14,2},{1,13},{3,15... | collective-permute-start | bytes 196616 | tf_op jit(solution)/shard_map/ppermute | solution.py:24
  58.9 3.6 %collective-permute-start.15 = (f32[32]{0:T(128)S(1)}, f32[32]{0:T(128)S(1)}, u32[]{:S(2)}, u32[]{:S(2)}) collective-permute-start(f32[32]{0:T(128)S(1)} %get-tuple-element.5), channel_id=1, source_target_pairs={{0,1},{1,0},{2,3},{3,2},{4,5},{5,4},{6,7},{7,6},{8,9},{9,8},{10,11... | collective-permute-start | bytes 392 | tf_op jit(solution)/shard_map/ppermute | solution.py:27

commit v2 on v1

v2 whole, which is shorter than its diff:
```python
import jax
import jax.numpy as jnp
from jax import lax
from jax.experimental import pallas as pl
from jax.experimental.pallas import tpu as pltpu
from jax.sharding import PartitionSpec as P

EPSILON = 1e-06
LANES = 128


def fetch_body(tie, gate, up, down, gate_out, up_out, down_out, sems):
    copies = [
        pltpu.make_async_copy(gate.at[0], gate_out, sems.at[0]),
        pltpu.make_async_copy(up.at[0], up_out, sems.at[1]),
        pltpu.make_async_copy(down.at[0], down_out, sems.at[2]),
    ]
    for copy in copies:
        copy.start()
    for copy in copies:
        copy.wait()


def fetch(tie, gate, up, down):
    hbm = pl.BlockSpec(memory_space=pltpu.HBM)
    gate, up, down = [pltpu.with_memory_space_constraint(w, pltpu.HBM) for w in (gate, up, down)]
    vmem = pl.BlockSpec(memory_space=pltpu.VMEM)
    return pl.pallas_call(
        fetch_body,
        in_specs=[vmem, hbm, hbm, hbm],
        out_specs=[vmem, vmem, vmem],
        out_shape=[pltpu.VMEM(w.shape[1:], w.dtype) for w in (gate, up, down)],
        scratch_shapes=[pltpu.SemaphoreType.DMA((3,))],
        cost_estimate=pl.CostEstimate(
            flops=4 * 10**9, transcendentals=0, bytes_accessed=2 * (gate.size + up.size + down.size)
        ),
        compiler_params=pltpu.CompilerParams(vmem_limit_bytes=2 << 20),
        name="fetch_weights",
    )(tie, gate, up, down)


def expert_body(count, *refs):
    blocks = refs[:count]
    place, gate, up, down, away, home, tokens, hidden = refs[count:]
    rows = blocks[0].shape[0]
    width = gate.shape[0]
    ff = gate.shape[1]
    step = min(256, ff)
    for i in range(count):
        tokens[i * rows : (i + 1) * rows, :] = blocks[i][...]
    lanes = tokens[:, width:].astype(jnp.float32)
    mix = jnp.sum(lanes * place[...], axis=1, keepdims=True)
    x = tokens[:, :width]
    for j in range(ff // step):
        cut = slice(j * step, (j + 1) * step)
        g = jnp.dot(x, gate[:, cut], preferred_element_type=jnp.float32)
        u = jnp.dot(x, up[:, cut], preferred_element_type=jnp.float32)
        hidden[:, cut] = (g / (1.0 + jnp.exp(-g)) * u * mix).astype(jnp.bfloat16)
    cutoff = away.shape[0]
    span = min(512, width)
    for j in range(width // span):
        cut = slice(j * span, (j + 1) * span)
        out = jnp.dot(hidden[...], down[:, cut], preferred_element_type=jnp.float32)
        away[:, cut] = out[:cutoff].astype(jnp.bfloat16)
        home[:, cut] = out[cutoff:]


def expert(blocks, place, gate, up, down):
    count = len(blocks)
    rows, wide = blocks[0].shape
    all_rows = count * rows
    gate, up, down = [pltpu.with_memory_space_constraint(w, pltpu.VMEM) for w in (gate, up, down)]
    width, ff = gate.shape
    vmem = pl.BlockSpec(memory_space=pltpu.VMEM)
    return pl.pallas_call(
        lambda *refs: expert_body(count, *refs),
        in_specs=[vmem] * (count + 4),
        out_specs=[vmem, vmem],
        out_shape=[
            jax.ShapeDtypeStruct((all_rows // 2, width), jnp.bfloat16),
            jax.ShapeDtypeStruct((all_rows // 2, width), jnp.float32),
        ],
        scratch_shapes=[
            pltpu.VMEM((all_rows, wide), jnp.bfloat16),
            pltpu.VMEM((all_rows, ff), jnp.bfloat16),
        ],
        cost_estimate=pl.CostEstimate(
            flops=6 * all_rows * width * ff, transcendentals=all_rows * ff, bytes_accessed=2 * all_rows * width
        ),
        compiler_params=pltpu.CompilerParams(vmem_limit_bytes=24 << 20),
        name="expert",
    )(*blocks, place, gate, up, down)


def step(
    tokens, routes, gates, norm_gain, exp_gate, exp_up, exp_down, sh_gate, sh_up, sh_down, out_gain
):
    ep = lax.axis_size("ep")
    tp = lax.axis_size("tp")
    assert tp & (tp - 1) == 0 and ep & (ep - 1) == 0 and exp_gate.shape[0] == 1
    rows, width = tokens.shape
    half = width // tp
    chips = ep // 2
    me = lax.axis_index("ep")
    side = lax.axis_index("tp")
    f32, bf16 = jnp.float32, jnp.bfloat16

    def across(x, bits):
        return lax.ppermute(x, "ep", [(i, i ^ bits) for i in range(ep)])

    def over_tp(x, bits):
        return lax.ppermute(x, "tp", [(i, i ^ bits) for i in range(tp)])

    def features(x, index):
        if tp == 2:
            return jnp.where(index == 0, x[..., :half], x[..., half:])
        return lax.dynamic_slice_in_dim(x, index * half, half, axis=x.ndim - 1)

    values = tokens.astype(f32)
    normed = (
        values
        * lax.rsqrt(jnp.mean(values * values, axis=1, keepdims=True) + EPSILON)
        * norm_gain.astype(f32)
    ).astype(bf16)
    extra = (2 * ep + LANES - 1) // LANES * LANES
    column = jnp.arange(extra, dtype=jnp.int32)
    weight = jnp.sum(
        jnp.where(routes[:, :, None] == (column % ep)[None, None, :], gates[:, :, None], 0.0), axis=1
    )
    coarse = weight.astype(bf16)
    fine = (weight - coarse.astype(f32)).astype(bf16)
    packed = jnp.where(column < ep, coarse, jnp.where(column < 2 * ep, fine, jnp.zeros((), bf16)))
    block = jnp.concatenate([normed, packed], axis=1)

    place = ((column % ep == me) & (column < 2 * ep)).astype(f32)[None, :]
    chosen = (jnp.arange(width, dtype=jnp.int32) // half == side)[None, :]
    block, place, chosen = lax.optimization_barrier((block, place, chosen))

    mine = [block]
    for k in range(1, chips):
        mine.append(across(block, 2 * k))
    theirs = [across(b, 1) for b in mine]

    shared_gate = jnp.dot(normed, sh_gate, preferred_element_type=f32)
    shared_up = jnp.dot(normed, sh_up, preferred_element_type=f32)
    shared_hidden = (jax.nn.silu(shared_gate) * shared_up).astype(bf16)
    shared_part = jnp.dot(shared_hidden, sh_down, preferred_element_type=f32)

    weights = fetch(block[:16, :LANES], exp_gate, exp_up, exp_down)
    away, home = expert(theirs + mine, place, *weights)
    other = across(away, 1)
    paired = [
        home[k * rows : (k + 1) * rows] + other[k * rows : (k + 1) * rows].astype(f32)
        for k in range(chips)
    ]
    total = paired[0] + shared_part
    moved = [across(paired[k].astype(bf16), 2 * k) for k in range(1, chips)]
    for piece in moved:
        total = total + piece.astype(f32)
    sent = total.astype(bf16)
    for bits in range(1, tp):
        total = total + over_tp(sent, bits).astype(f32)
    scale = lax.rsqrt(jnp.mean(total * total, axis=1) + EPSILON)
    if tp == 2:
        total = jnp.where(chosen[:, :half], total[:, :half], total[:, half:])
    else:
        total = features(total, side)
    return (total * scale[:, None] * out_gain.astype(f32)).astype(bf16)


def solution(mesh):
    placed = (
        P(("grp", "ep"), None),
        P(("grp", "ep"), None),
        P(("grp", "ep"), None),
        P(),
        P("ep", None, "tp"),
        P("ep", None, "tp"),
        P("ep", "tp", None),
        P(None, "tp"),
        P(None, "tp"),
        P("tp", None),
        P("tp"),
    )
    return jax.shard_map(
        step, mesh=mesh, in_specs=placed, out_specs=P(("grp", "ep"), "tp"), check_vma=False
    )
```

time: 63.6 us -> 55.2 us (0.87)
  matrix products: 16.2 us -> 3.58 us
  Pallas kernels: 0 us -> 8.24 us
  starting transfers between devices: 17.7 us -> 12.2 us
  waiting for transfers between devices: 19.6 us -> 24.1 us
  local copies, waits for them, and re-layouts: 1.9 us -> 0.04 us
  other arithmetic: 7.73 us -> 6.67 us
    dot_general x4 -> x2, matrix products: 16.2 us -> 3.58 us  [the longest x1 2.49 us: step(): shared_part = jnp.dot(shared_hidden, sh_down, preferred_element_type=f32)]
    pallas_call x0 -> x2, Pallas kernels: none -> 8.24 us  [the longest x1 4.68 us: fetch(): pl.pallas_call(fetch_body, in_specs=[vmem, hbm, hbm, hbm], out_specs=[vme...]
    ppermute x5 -> x1, starting transfers between devices: 5.73 us -> 1.55 us  [over_tp(): return lax.ppermute(x, 'tp', [(i, i ^ bits) for i in range(tp)])]
    ppermute x11, waiting for transfers between devices: 16.8 us -> 20.5 us  [across(): return lax.ppermute(x, 'ep', [(i, i ^ bits) for i in range(ep)])]
    add x1 -> x0, other arithmetic: 1.33 us -> none  [shards(): paired = part[chips * rows:].astype(f32) + other.astype(f32)]
    ppermute x11, starting transfers between devices: 12 us -> 10.7 us  [across(): return lax.ppermute(x, 'ep', [(i, i ^ bits) for i in range(ep)])]
    unnamed x14 -> x8, local copies, waits for them, and re-layouts: 0.99 us -> 0.02 us
    slice x1 -> x2, local copies, waits for them, and re-layouts: 0.89 us -> 0.03 us  [the longest x1 0.02 us: step(): total = jnp.where(chosen[:, :half], total[:, :half], total[:, half:])]
  transfers between devices with their start and end apart: 16 -> 12, of which waited for: 7 -> 7; matrix products, arithmetic and copies ran while one was open for 10% -> 7% of each run, Pallas kernels for 0% -> 9%
where the time goes in v2:
time: 55.2 us; the launch traced here: 55 us
  waiting for transfers between devices  24.1 us (44%)
  starting transfers between devices  12.2 us (22%)
  Pallas kernels  8.24 us (15%)
  other arithmetic  6.67 us (12%)
  matrix products  3.58 us (6%)
    ppermute x11, waiting for transfers between devices, across(): return lax.ppermute(x, 'ep', [(i, i ^ bits) for i in range(ep)])  20.5 us
    ppermute x11, starting transfers between devices, across(): return lax.ppermute(x, 'ep', [(i, i ^ bits) for i in range(ep)])  10.7 us
    pallas_call x1, Pallas kernels, fetch(): pl.pallas_call(fetch_body, in_specs=[vmem, hbm, hbm, hbm], out_specs=[vme...  4.68 us
    ppermute x1, waiting for transfers between devices, over_tp(): return lax.ppermute(x, 'tp', [(i, i ^ bits) for i in range(tp)])  3.58 us
    pallas_call x1, Pallas kernels, expert(): pl.pallas_call(lambda *refs: expert_body(count, *refs), in_specs=[vmem] *...  3.55 us
    dot_general x1, matrix products, step(): shared_part = jnp.dot(shared_hidden, sh_down, preferred_element_type=f32)  2.49 us
    ppermute x1, starting transfers between devices, over_tp(): return lax.ppermute(x, 'tp', [(i, i ^ bits) for i in range(tp)])  1.55 us
    convert_element_type x1, other arithmetic, step(): sent = total.astype(bf16)  1.18 us
  transfers between devices with their start and end apart: 12, of which 7 were waited for; matrix products, arithmetic and copies ran while one was open for 7% of the time, Pallas kernels for 9%

profile of v2, /device:TPU:0, one launch (start us, length us, event | category | flops | bytes accessed | tf_op | source)
XLA Modules:
  0.0 55.0 jit_solution(6574890947491071075)
XLA Ops:
  0.0 0.0 copy-start
  0.0 0.8 %convert_element_type.74 = f32[2048]{0:T(1024)S(1)} convert(bf16[2048]{0:T(1024)(128)(2,1)} %param.14) | non-fusion elementwise | flops 2048 | bytes 12288 | tf_op jit(solution)/shard_map/convert_element_type | solution.py:123
  0.9 1.0 %fusion.2 = f32[32]{0:T(128)S(1)} fusion(bf16[32,2048]{1,0:T(8,128)(2,1)} %param.11), kind=kLoop, calls=%fused_computation.5 | loop fusion | flops 196576 | bytes 131200 | tf_op jit(solution)/shard_map/reduce_sum | solution.py:122
  2.0 1.0 %fusion.4 = bf16[32,2048]{1,0:T(8,128)(2,1)S(1)} fusion(bf16[32,2048]{1,0:T(8,128)(2,1)} %param.11, f32[2048]{0:T(1024)S(1)} %convert_element_type.74, f32[32]{0:T(128)S(1)} %add_rsqrt_fusion.1), kind=kLoop, calls=%fused_computation.7 | loop fusion | flops 262144 | bytes 270464 | tf_op jit(solution)/shard_map/convert_element_type | solution.py:124
  3.0 0.8 %select_reduce_fusion = f32[32,128]{1,0:T(8,128)S(1)} fusion(f32[32,4]{0,1:T(4,128)} %param.13, s32[128]{0:T(128)S(1)} %and_select_fusion.2, s32[32,4]{0,1:T(4,128)} %param.12), kind=kLoop, calls=%fused_computation.24 | loop fusion | flops 45056 | bytes 17920 | tf_op jit(solution)/shard_map/reduce_sum | solution.py:127
  3.8 3.1 %collective-permute-start.1 = (bf16[32,2176]{1,0:T(8,128)(2,1)S(1)}, bf16[32,2176]{1,0:T(8,128)(2,1)S(1)}, u32[]{:S(2)}, u32[]{:S(2)}) collective-permute-start(bf16[32,2176]{1,0:T(8,128)(2,1)S(1)} %pad_maximum_fusion.refs_4_), channel_id=1, source_target_pairs={{0,4},{2,6},{4,0},{6,2},{8,12},{10,14},{12,8},{14,10},{1,5},{3,7},... | collective-permute-start | bytes 417800 | tf_op jit(solution)/shard_map/ppermute | solution.py:109
  6.9 2.6 %collective-permute-start.3 = (bf16[32,2176]{1,0:T(8,128)(2,1)S(1)}, bf16[32,2176]{1,0:T(8,128)(2,1)S(1)}, u32[]{:S(2)}, u32[]{:S(2)}) collective-permute-start(bf16[32,2176]{1,0:T(8,128)(2,1)S(1)} %pad_maximum_fusion.refs_4_), channel_id=1, source_target_pairs={{0,8},{2,10},{4,12},{6,14},{8,0},{10,2},{12,4},{14,6},{1,9},{3,11}... | collective-permute-start | bytes 417800 | tf_op jit(solution)/shard_map/ppermute | solution.py:109
  9.5 0.0 collective-permute-start.5
  9.5 0.0 collective-permute-start
  9.5 2.9 %collective-permute-done.1.refs_5_ = bf16[32,2176]{1,0:T(8,128)(2,1)S(1)} collective-permute-done((bf16[32,2176]{1,0:T(8,128)(2,1)S(1)}, bf16[32,2176]{1,0:T(8,128)(2,1)S(1)}, u32[]{:S(2)}, u32[]{:S(2)}) %collective-permute-start.1) | collective-permute-done | bytes 139296 | tf_op jit(solution)/shard_map/ppermute | solution.py:109
  12.4 0.0 collective-permute-start.2
  12.4 7.9 %collective-permute-done.3.refs_6_ = bf16[32,2176]{1,0:T(8,128)(2,1)S(1)} collective-permute-done((bf16[32,2176]{1,0:T(8,128)(2,1)S(1)}, bf16[32,2176]{1,0:T(8,128)(2,1)S(1)}, u32[]{:S(2)}, u32[]{:S(2)}) %collective-permute-start.3) | collective-permute-done | bytes 139296 | tf_op jit(solution)/shard_map/ppermute | solution.py:109
  20.3 0.0 collective-permute-start.4
  20.3 0.0 collective-permute-done.5.refs_7_
  20.3 0.5 collective-permute-start.6
  20.9 4.7 %fetch_weights.1 = (bf16[2048,1024]{1,0:T(8,128)(2,1)S(1)}, bf16[2048,1024]{1,0:T(8,128)(2,1)S(1)}, bf16[1024,2048]{1,0:T(8,128)(2,1)S(1)}) custom-call(bf16[16,128]{1,0:T(8,128)(2,1)S(1)} %slice.37.tie, bf16[1,2048,1024]{2,1,0:T(8,128)(2,1)} %gate.1, bf16[1,2048,1024]{2,1,0:T(8,128)(2,1)} %up.1, bf16[1,1024,2048]{2,1,0:T(8,128)(2,1)} %down.1), custom_call_target="tpu_custom_call" | custom-call | flops 4000000000 | bytes 12582912 | tf_op jit(solution)/shard_map/fetch_weights/pallas_call | solution.py:28
  25.5 0.0 collective-permute-done.refs_0_
  25.6 0.0 collective-permute-done.2.refs_1_
  25.6 0.0 collective-permute-done.4.refs_2_
  25.6 0.0 collective-permute-done.6.refs_3_
  25.6 0.0 copy-start.1
  25.6 3.6 %expert.1 = (bf16[128,2048]{1,0:T(8,128)(2,1)S(1)}, f32[128,2048]{1,0:T(8,128)S(1)}) custom-call(bf16[32,2176]{1,0:T(8,128)(2,1)S(1)} %collective-permute-done.refs_0_, bf16[32,2176]{1,0:T(8,128)(2,1)S(1)} %collective-permute-done.2.refs_1_, bf16[32,2176]{1,0:T(8,128)(2,1)S(1)} %collective-permute-done.4.refs_2_, ...), custom_call_target="tpu_custom_call" | custom-call | flops 3221225472 | bytes 1048576 | tf_op jit(solution)/shard_map/expert/pallas_call | solution.py:75
  29.2 0.1 collective-permute-start.7
  29.2 0.0 copy-done.1
  29.2 1.1 %fusion.19 = f32[32,512]{1,0:T(8,128)} fusion(bf16[32,2048]{1,0:T(8,128)(2,1)S(1)} %fusion.4, bf16[2048,512]{1,0:T(8,128)(2,1)S(1)} %copy-done.1), kind=kOutput, calls=%fused_computation.44 | convolution fusion | flops 67108864 | bytes 2293760 | tf_op jit(solution)/shard_map/dot_general | solution.py:144
  30.3 0.8 %collective-permute-done.7 = bf16[128,2048]{1,0:T(8,128)(2,1)S(1)} collective-permute-done((bf16[128,2048]{1,0:T(8,128)(2,1)S(1)}, bf16[128,2048]{1,0:T(8,128)(2,1)S(1)}, u32[]{:S(2)}, u32[]{:S(2)}) %collective-permute-start.7) | collective-permute-done | bytes 524320 | tf_op jit(solution)/shard_map/ppermute | solution.py:109
  31.1 0.0 copy-start.2
  31.1 0.9 %add_convert_fusion.2 = (bf16[32,2048]{1,0:T(8,128)(2,1)}, bf16[32,2048]{1,0:T(8,128)(2,1)}, bf16[32,2048]{1,0:T(8,128)(2,1)}) fusion(f32[128,2048]{1,0:T(8,128)S(1)} %get-tuple-element.19, bf16[128,2048]{1,0:T(8,128)(2,1)S(1)} %collective-permute-done.7), kind=kLoop, calls=%fused_computation.13 | loop fusion | flops 589824 | bytes 1572864 | tf_op jit(solution)/shard_map/convert_element_type | solution.py:157
  32.0 2.3 %collective-permute-start.10 = (bf16[32,2048]{1,0:T(8,128)(2,1)}, bf16[32,2048]{1,0:T(8,128)(2,1)}, u32[]{:S(2)}, u32[]{:S(2)}) collective-permute-start(bf16[32,2048]{1,0:T(8,128)(2,1)} %get-tuple-element.26), channel_id=1, source_target_pairs={{0,12},{2,14},{4,8},{6,10},{8,4},{10,6},{12,0},{14,2},{1,13},{3,15... | collective-permute-start | bytes 393224 | tf_op jit(solution)/shard_map/ppermute | solution.py:109
  34.3 1.1 %collective-permute-start.8 = (bf16[32,2048]{1,0:T(8,128)(2,1)}, bf16[32,2048]{1,0:T(8,128)(2,1)}, u32[]{:S(2)}, u32[]{:S(2)}) collective-permute-start(bf16[32,2048]{1,0:T(8,128)(2,1)} %get-tuple-element.25), channel_id=1, source_target_pairs={{0,4},{2,6},{4,0},{6,2},{8,12},{10,14},{12,8},{14,10},{1,5},{3,7},... | collective-permute-start | bytes 393224 | tf_op jit(solution)/shard_map/ppermute | solution.py:109
  35.4 0.0 copy-done.2
  35.4 0.0 copy-start.3
  35.4 1.0 %collective-permute-start.9 = (bf16[32,2048]{1,0:T(8,128)(2,1)}, bf16[32,2048]{1,0:T(8,128)(2,1)}, u32[]{:S(2)}, u32[]{:S(2)}) collective-permute-start(bf16[32,2048]{1,0:T(8,128)(2,1)} %get-tuple-element.27), channel_id=1, source_target_pairs={{0,8},{2,10},{4,12},{6,14},{8,0},{10,2},{12,4},{14,6},{1,9},{3,11}... | collective-permute-start | bytes 393224 | tf_op jit(solution)/shard_map/ppermute | solution.py:109
  36.4 0.0 copy-done
  36.4 2.5 %fusion.1 = f32[32,2048]{1,0:T(8,128)S(1)} fusion(bf16[512,2048]{1,0:T(8,128)(2,1)S(1)} %copy-done, bf16[32,2048]{1,0:T(8,128)(2,1)S(1)} %fusion.4, bf16[2048,512]{1,0:T(8,128)(2,1)} %param.19, f32[32,512]{1,0:T(8,128)} %fusion.19), kind=kOutput, calls=%fused_computation.2 | convolution fusion | flops 134316032 | bytes 4653056 | tf_op jit(solution)/shard_map/dot_general | solution.py:147
  38.9 1.6 %collective-permute-done.10 = bf16[32,2048]{1,0:T(8,128)(2,1)} collective-permute-done((bf16[32,2048]{1,0:T(8,128)(2,1)}, bf16[32,2048]{1,0:T(8,128)(2,1)}, u32[]{:S(2)}, u32[]{:S(2)}) %collective-permute-start.10) | collective-permute-done | bytes 131104 | tf_op jit(solution)/shard_map/ppermute | solution.py:109
  40.5 2.3 %collective-permute-done.8 = bf16[32,2048]{1,0:T(8,128)(2,1)} collective-permute-done((bf16[32,2048]{1,0:T(8,128)(2,1)}, bf16[32,2048]{1,0:T(8,128)(2,1)}, u32[]{:S(2)}, u32[]{:S(2)}) %collective-permute-start.8) | collective-permute-done | bytes 131104 | tf_op jit(solution)/shard_map/ppermute | solution.py:109
  42.8 4.9 %collective-permute-done.9 = bf16[32,2048]{1,0:T(8,128)(2,1)} collective-permute-done((bf16[32,2048]{1,0:T(8,128)(2,1)}, bf16[32,2048]{1,0:T(8,128)(2,1)}, u32[]{:S(2)}, u32[]{:S(2)}) %collective-permute-start.9) | collective-permute-done | bytes 131104 | tf_op jit(solution)/shard_map/ppermute | solution.py:109
  47.8 1.2 %fusion.18 = (bf16[32,2048]{1,0:T(8,128)(2,1)S(1)}, f32[32,2048]{1,0:T(8,128)S(1)}) fusion(bf16[32,2048]{1,0:T(8,128)(2,1)} %collective-permute-done.10, bf16[32,2048]{1,0:T(8,128)(2,1)} %collective-permute-done.9, bf16[32,2048]{1,0:T(8,128)(2,1)} %collective-permute-done.8, f32[32,2048]{1,0:T(8,128)S(1)} %fusion.1, bf16[128,2048]{1,0:T(8,128)(2,1)} %copy-done.2, ...), kind=kLoop, calls=%fused_computation.43 | loop fusion | flops 655360 | bytes 1441792 | tf_op jit(solution)/shard_map/convert_element_type | solution.py:160
  49.0 1.6 %collective-permute-start.11 = (bf16[32,2048]{1,0:T(8,128)(2,1)S(1)}, bf16[32,2048]{1,0:T(8,128)(2,1)S(1)}, u32[]{:S(2)}, u32[]{:S(2)}) collective-permute-start(bf16[32,2048]{1,0:T(8,128)(2,1)S(1)} %get-tuple-element.23), channel_id=1, source_target_pairs={{0,1},{1,0},{2,3},{3,2},{4,5},{5,4},{6,7},{7,6},{8,9},{9,8},{10,11... | collective-permute-start | bytes 393224 | tf_op jit(solution)/shard_map/ppermute | solution.py:112
  50.5 0.0 copy-done.3
  50.5 3.6 %collective-permute-done.11 = bf16[32,2048]{1,0:T(8,128)(2,1)S(1)} collective-permute-done((bf16[32,2048]{1,0:T(8,128)(2,1)S(1)}, bf16[32,2048]{1,0:T(8,128)(2,1)S(1)}, u32[]{:S(2)}, u32[]{:S(2)}) %collective-permute-start.11) | collective-permute-done | bytes 131104 | tf_op jit(solution)/shard_map/ppermute | solution.py:112
  54.1 0.1 multiply_reduce_fusion
  54.3 0.7 %fusion.7 = bf16[32,1024]{1,0:T(8,128)(2,1)} fusion(f32[32,2048]{1,0:T(8,128)S(1)} %get-tuple-element.22, f32[1024]{0:T(1024)S(1)} %convert_element_type.93, f32[32]{0:T(128)S(1)} %add_rsqrt_fusion, pred[1024]{0:T(1024)(128)(4,1)S(1)} %slice_reduce_fusion), kind=kLoop, calls=%fused_computation.18 | loop fusion | flops 131072 | bytes 332928 | tf_op jit(solution)/shard_map/convert_element_type | solution.py:168
  (11 shorter events, 0.1 us)
Async XLA Ops:
  0.0 36.4 %copy-start = (bf16[512,2048]{1,0:T(8,128)(2,1)S(1)}, bf16[512,2048]{1,0:T(8,128)(2,1)}, u32[]{:S(2)}) copy-start(bf16[512,2048]{1,0:T(8,128)(2,1)} %param.20) | copy-start | bytes 6291460
  3.8 8.6 %collective-permute-start.1 = (bf16[32,2176]{1,0:T(8,128)(2,1)S(1)}, bf16[32,2176]{1,0:T(8,128)(2,1)S(1)}, u32[]{:S(2)}, u32[]{:S(2)}) collective-permute-start(bf16[32,2176]{1,0:T(8,128)(2,1)S(1)} %pad_maximum_fusion.refs_4_), channel_id=1, source_target_pairs={{0,4},{2,6},{4,0},{6,2},{8,12},{10,14},{12,8},{14,10},{1,5},{3,7},... | collective-permute-start | bytes 417800 | tf_op jit(solution)/shard_map/ppermute | solution.py:109
  6.9 13.4 %collective-permute-start.3 = (bf16[32,2176]{1,0:T(8,128)(2,1)S(1)}, bf16[32,2176]{1,0:T(8,128)(2,1)S(1)}, u32[]{:S(2)}, u32[]{:S(2)}) collective-permute-start(bf16[32,2176]{1,0:T(8,128)(2,1)S(1)} %pad_maximum_fusion.refs_4_), channel_id=1, source_target_pairs={{0,8},{2,10},{4,12},{6,14},{8,0},{10,2},{12,4},{14,6},{1,9},{3,11}... | collective-permute-start | bytes 417800 | tf_op jit(solution)/shard_map/ppermute | solution.py:109
  9.5 10.8 %collective-permute-start.5 = (bf16[32,2176]{1,0:T(8,128)(2,1)S(1)}, bf16[32,2176]{1,0:T(8,128)(2,1)S(1)}, u32[]{:S(2)}, u32[]{:S(2)}) collective-permute-start(bf16[32,2176]{1,0:T(8,128)(2,1)S(1)} %pad_maximum_fusion.refs_4_), channel_id=1, source_target_pairs={{0,12},{2,14},{4,8},{6,10},{8,4},{10,6},{12,0},{14,2},{1,13},{3,15... | collective-permute-start | bytes 417800 | tf_op jit(solution)/shard_map/ppermute | solution.py:109
  9.5 16.0 %collective-permute-start = (bf16[32,2176]{1,0:T(8,128)(2,1)S(1)}, bf16[32,2176]{1,0:T(8,128)(2,1)S(1)}, u32[]{:S(2)}, u32[]{:S(2)}) collective-permute-start(bf16[32,2176]{1,0:T(8,128)(2,1)S(1)} %pad_maximum_fusion.refs_4_), channel_id=1, source_target_pairs={{0,2},{2,0},{4,6},{6,4},{8,10},{10,8},{12,14},{14,12},{1,3},{3,1},... | collective-permute-start | bytes 417800 | tf_op jit(solution)/shard_map/ppermute | solution.py:109
  12.4 13.1 %collective-permute-start.2 = (bf16[32,2176]{1,0:T(8,128)(2,1)S(1)}, bf16[32,2176]{1,0:T(8,128)(2,1)S(1)}, u32[]{:S(2)}, u32[]{:S(2)}) collective-permute-start(bf16[32,2176]{1,0:T(8,128)(2,1)S(1)} %collective-permute-done.1.refs_5_), channel_id=1, source_target_pairs={{0,2},{2,0},{4,6},{6,4},{8,10},{10,8},{12,14},{14,12},{1,3},{3,1},... | collective-permute-start | bytes 417800 | tf_op jit(solution)/shard_map/ppermute | solution.py:109
  20.3 5.2 %collective-permute-start.4 = (bf16[32,2176]{1,0:T(8,128)(2,1)S(1)}, bf16[32,2176]{1,0:T(8,128)(2,1)S(1)}, u32[]{:S(2)}, u32[]{:S(2)}) collective-permute-start(bf16[32,2176]{1,0:T(8,128)(2,1)S(1)} %collective-permute-done.3.refs_6_), channel_id=1, source_target_pairs={{0,2},{2,0},{4,6},{6,4},{8,10},{10,8},{12,14},{14,12},{1,3},{3,1},... | collective-permute-start | bytes 417800 | tf_op jit(solution)/shard_map/ppermute | solution.py:109
  20.3 5.2 %collective-permute-start.6 = (bf16[32,2176]{1,0:T(8,128)(2,1)S(1)}, bf16[32,2176]{1,0:T(8,128)(2,1)S(1)}, u32[]{:S(2)}, u32[]{:S(2)}) collective-permute-start(bf16[32,2176]{1,0:T(8,128)(2,1)S(1)} %collective-permute-done.5.refs_7_), channel_id=1, source_target_pairs={{0,2},{2,0},{4,6},{6,4},{8,10},{10,8},{12,14},{14,12},{1,3},{3,1},... | collective-permute-start | bytes 417800 | tf_op jit(solution)/shard_map/ppermute | solution.py:109
  25.6 3.7 %copy-start.1 = (bf16[2048,512]{1,0:T(8,128)(2,1)S(1)}, bf16[2048,512]{1,0:T(8,128)(2,1)}, u32[]{:S(2)}) copy-start(bf16[2048,512]{1,0:T(8,128)(2,1)} %param.18) | copy-start | bytes 6291460
  29.2 2.0 %collective-permute-start.7 = (bf16[128,2048]{1,0:T(8,128)(2,1)S(1)}, bf16[128,2048]{1,0:T(8,128)(2,1)S(1)}, u32[]{:S(2)}, u32[]{:S(2)}) collective-permute-start(bf16[128,2048]{1,0:T(8,128)(2,1)S(1)} %get-tuple-element.20), channel_id=1, source_target_pairs={{0,2},{2,0},{4,6},{6,4},{8,10},{10,8},{12,14},{14,12},{1,3},{3,1},... | collective-permute-start | bytes 1572872 | tf_op jit(solution)/shard_map/ppermute | solution.py:109
  31.1 4.3 %copy-start.2 = (bf16[128,2048]{1,0:T(8,128)(2,1)}, bf16[128,2048]{1,0:T(8,128)(2,1)S(1)}, u32[]{:S(2)}) copy-start(bf16[128,2048]{1,0:T(8,128)(2,1)S(1)} %collective-permute-done.7) | copy-start | bytes 1572868
  32.0 8.5 %collective-permute-start.10 = (bf16[32,2048]{1,0:T(8,128)(2,1)}, bf16[32,2048]{1,0:T(8,128)(2,1)}, u32[]{:S(2)}, u32[]{:S(2)}) collective-permute-start(bf16[32,2048]{1,0:T(8,128)(2,1)} %get-tuple-element.26), channel_id=1, source_target_pairs={{0,12},{2,14},{4,8},{6,10},{8,4},{10,6},{12,0},{14,2},{1,13},{3,15... | collective-permute-start | bytes 393224 | tf_op jit(solution)/shard_map/ppermute | solution.py:109
  34.3 8.6 %collective-permute-start.8 = (bf16[32,2048]{1,0:T(8,128)(2,1)}, bf16[32,2048]{1,0:T(8,128)(2,1)}, u32[]{:S(2)}, u32[]{:S(2)}) collective-permute-start(bf16[32,2048]{1,0:T(8,128)(2,1)} %get-tuple-element.25), channel_id=1, source_target_pairs={{0,4},{2,6},{4,0},{6,2},{8,12},{10,14},{12,8},{14,10},{1,5},{3,7},... | collective-permute-start | bytes 393224 | tf_op jit(solution)/shard_map/ppermute | solution.py:109
  35.4 15.1 %copy-start.3 = (bf16[1024]{0:T(1024)(128)(2,1)S(1)}, bf16[1024]{0:T(1024)(128)(2,1)}, u32[]{:S(2)}) copy-start(bf16[1024]{0:T(1024)(128)(2,1)} %param.21) | copy-start | bytes 6148
  35.4 12.4 %collective-permute-start.9 = (bf16[32,2048]{1,0:T(8,128)(2,1)}, bf16[32,2048]{1,0:T(8,128)(2,1)}, u32[]{:S(2)}, u32[]{:S(2)}) collective-permute-start(bf16[32,2048]{1,0:T(8,128)(2,1)} %get-tuple-element.27), channel_id=1, source_target_pairs={{0,8},{2,10},{4,12},{6,14},{8,0},{10,2},{12,4},{14,6},{1,9},{3,11}... | collective-permute-start | bytes 393224 | tf_op jit(solution)/shard_map/ppermute | solution.py:109
  49.0 5.2 %collective-permute-start.11 = (bf16[32,2048]{1,0:T(8,128)(2,1)S(1)}, bf16[32,2048]{1,0:T(8,128)(2,1)S(1)}, u32[]{:S(2)}, u32[]{:S(2)}) collective-permute-start(bf16[32,2048]{1,0:T(8,128)(2,1)S(1)} %get-tuple-element.23), channel_id=1, source_target_pairs={{0,1},{1,0},{2,3},{3,2},{4,5},{5,4},{6,7},{7,6},{8,9},{9,8},{10,11... | collective-permute-start | bytes 393224 | tf_op jit(solution)/shard_map/ppermute | solution.py:112

commit v3 on v2

--- a/solution.py
+++ b/solution.py
@@ -7,6 +7,35 @@
 
 EPSILON = 1e-06
 LANES = 128
+
+
+def prepare_body(ep, tokens, routes, gates, gain, out):
+    width = tokens.shape[1]
+    values = tokens[...].astype(jnp.float32)
+    scale = lax.rsqrt(jnp.mean(values * values, axis=1, keepdims=True) + EPSILON)
+    out[:, :width] = (values * scale * gain[...].astype(jnp.float32)).astype(jnp.bfloat16)
+    shape = (tokens.shape[0], out.shape[1] - width)
+    column = lax.broadcasted_iota(jnp.int32, shape, 1)
+    name = jnp.where(column < ep, column, column - ep)
+    weight = jnp.zeros(shape, jnp.float32)
+    for k in range(routes.shape[1]):
+        weight = weight + jnp.where(name == routes[:, k : k + 1], gates[:, k : k + 1], 0.0)
+    coarse = weight.astype(jnp.bfloat16).astype(jnp.float32)
+    packed = jnp.where(column < ep, coarse, jnp.where(column < 2 * ep, weight - coarse, 0.0))
+    out[:, width:] = packed.astype(jnp.bfloat16)
+
+
+def prepare(tokens, routes, gates, gain, ep, extra):
+    rows, width = tokens.shape
+    vmem = pl.BlockSpec(memory_space=pltpu.VMEM)
+    return pl.pallas_call(
+        lambda *refs: prepare_body(ep, *refs),
+        in_specs=[vmem] * 4,
+        out_specs=vmem,
+        out_shape=jax.ShapeDtypeStruct((rows, width + extra), jnp.bfloat16),
+        compiler_params=pltpu.CompilerParams(vmem_limit_bytes=8 << 20),
+        name="prepare",
+    )(tokens, routes, gates, gain[None, :])
 
 
 def fetch_body(tie, gate, up, down, gate_out, up_out, down_out, sems):
@@ -116,22 +145,10 @@
             return jnp.where(index == 0, x[..., :half], x[..., half:])
         return lax.dynamic_slice_in_dim(x, index * half, half, axis=x.ndim - 1)
 
-    values = tokens.astype(f32)
-    normed = (
-        values
-        * lax.rsqrt(jnp.mean(values * values, axis=1, keepdims=True) + EPSILON)
-        * norm_gain.astype(f32)
-    ).astype(bf16)
     extra = (2 * ep + LANES - 1) // LANES * LANES
     column = jnp.arange(extra, dtype=jnp.int32)
-    weight = jnp.sum(
-        jnp.where(routes[:, :, None] == (column % ep)[None, None, :], gates[:, :, None], 0.0), axis=1
-    )
-    coarse = weight.astype(bf16)
-    fine = (weight - coarse.astype(f32)).astype(bf16)
-    packed = jnp.where(column < ep, coarse, jnp.where(column < 2 * ep, fine, jnp.zeros((), bf16)))
-    block = jnp.concatenate([normed, packed], axis=1)
-
+    block = prepare(tokens, routes, gates, norm_gain, ep, extra)
+    normed = block[:, :width]
     place = ((column % ep == me) & (column < 2 * ep)).astype(f32)[None, :]
     chosen = (jnp.arange(width, dtype=jnp.int32) // half == side)[None, :]
     block, place, chosen = lax.optimization_barrier((block, place, chosen))

time: 55.2 us -> 55 us (level)
  local copies, waits for them, and re-layouts: 0.04 us -> 3.3 us
  other arithmetic: 6.67 us -> 3.67 us
  waiting for transfers between devices: 24.1 us -> 23.4 us
    unnamed x8 -> x10, local copies, waits for them, and re-layouts: 0.02 us -> 2.59 us
    convert_element_type x2 -> x0, other arithmetic: 1.84 us -> none  [the longest x1 1 us: step(): normed = (values * lax.rsqrt(jnp.mean(values * values, axis=1, keepdims=T...]
    reduce_sum x2 -> x0, other arithmetic: 1.83 us -> none  [the longest x1 1.04 us: step(): jnp.mean(values * values, axis=1, keepdims=True) + EPSILON]
    broadcast_in_dim x0 -> x1, local copies, waits for them, and re-layouts: none -> 0.69 us  [prepare(): gain[None, :]]
    ppermute x1, waiting for transfers between devices: 3.58 us -> 2.9 us  [over_tp(): return lax.ppermute(x, 'tp', [(i, i ^ bits) for i in range(tp)])]
    convert_element_type x2, other arithmetic: 0.72 us -> 1.4 us  [step(): return (total * scale[:, None] * out_gain.astype(f32)).astype(bf16)]
  transfers between devices with their start and end apart: 12 -> 12, of which waited for: 7 -> 7; matrix products, arithmetic and copies ran while one was open for 7% -> 8% of each run, Pallas kernels for 9% -> 9%
where the time goes in v3:
time: 55 us; the launch traced here: 54.7 us
  waiting for transfers between devices  23.4 us (43%)
  starting transfers between devices  12.2 us (22%)
  Pallas kernels  8.4 us (15%)
  other arithmetic  3.67 us (7%)
  matrix products  3.58 us (7%)
  local copies, waits for them, and re-layouts  3.3 us (6%)
    ppermute x11, waiting for transfers between devices, across(): return lax.ppermute(x, 'ep', [(i, i ^ bits) for i in range(ep)])  20.5 us
    ppermute x11, starting transfers between devices, across(): return lax.ppermute(x, 'ep', [(i, i ^ bits) for i in range(ep)])  10.7 us
    pallas_call x1, Pallas kernels, fetch(): pl.pallas_call(fetch_body, in_specs=[vmem, hbm, hbm, hbm], out_specs=[vme...  4.68 us
    pallas_call x1, Pallas kernels, expert(): pl.pallas_call(lambda *refs: expert_body(count, *refs), in_specs=[vmem] *...  3.57 us
    ppermute x1, waiting for transfers between devices, over_tp(): return lax.ppermute(x, 'tp', [(i, i ^ bits) for i in range(tp)])  2.9 us
    unnamed x10, local copies, waits for them, and re-layouts  2.59 us
    dot_general x1, matrix products, step(): shared_part = jnp.dot(shared_hidden, sh_down, preferred_element_type=f32)  2.49 us
    ppermute x1, starting transfers between devices, over_tp(): return lax.ppermute(x, 'tp', [(i, i ^ bits) for i in range(tp)])  1.55 us
  transfers between devices with their start and end apart: 12, of which 7 were waited for; matrix products, arithmetic and copies ran while one was open for 8% of the time, Pallas kernels for 9%

profile of v3, /device:TPU:0, one launch (start us, length us, event | category | flops | bytes accessed | tf_op | source)
XLA Modules:
  0.0 54.7 jit_solution(2156669632155269098)
XLA Ops:
  0.0 0.0 copy-start
  0.0 0.9 %copy.12.refs_1_ = s32[32,4]{1,0:T(8,128)S(1)} copy(s32[32,4]{0,1:T(4,128)} %param.12) | data formatting | bytes 1024 | tf_op args[1]
  0.9 0.8 %copy.13.refs_2_ = f32[32,4]{1,0:T(8,128)S(1)} copy(f32[32,4]{0,1:T(4,128)} %param.13) | data formatting | bytes 1024 | tf_op args[2]
  1.7 0.7 %broadcast_in_dim.17.refs_3_ = bf16[1,2048]{1,0:T(2,128)(2,1)S(1)} reshape(bf16[2048]{0:T(1024)(128)(2,1)} %param.14) | data formatting | bytes 8192 | tf_op jit(solution)/shard_map/broadcast_in_dim | solution.py:38
  2.4 0.0 copy-start.1
  2.4 0.9 %copy-done.1 = bf16[32,2048]{1,0:T(8,128)(2,1)S(1)} copy-done((bf16[32,2048]{1,0:T(8,128)(2,1)S(1)}, bf16[32,2048]{1,0:T(8,128)(2,1)}, u32[]{:S(2)}) %copy-start.1) | copy-done | bytes 131096
  3.3 0.2 prepare.1.refs_4_
  3.5 3.1 %collective-permute-start.1 = (bf16[32,2176]{1,0:T(8,128)(2,1)S(1)}, bf16[32,2176]{1,0:T(8,128)(2,1)S(1)}, u32[]{:S(2)}, u32[]{:S(2)}) collective-permute-start(bf16[32,2176]{1,0:T(8,128)(2,1)S(1)} %prepare.1.refs_4_), channel_id=1, source_target_pairs={{0,4},{2,6},{4,0},{6,2},{8,12},{10,14},{12,8},{14,10},{1,5},{3,7},... | collective-permute-start | bytes 417800 | tf_op jit(solution)/shard_map/ppermute | solution.py:138
  6.6 2.6 %collective-permute-start.3 = (bf16[32,2176]{1,0:T(8,128)(2,1)S(1)}, bf16[32,2176]{1,0:T(8,128)(2,1)S(1)}, u32[]{:S(2)}, u32[]{:S(2)}) collective-permute-start(bf16[32,2176]{1,0:T(8,128)(2,1)S(1)} %prepare.1.refs_4_), channel_id=1, source_target_pairs={{0,8},{2,10},{4,12},{6,14},{8,0},{10,2},{12,4},{14,6},{1,9},{3,11}... | collective-permute-start | bytes 417800 | tf_op jit(solution)/shard_map/ppermute | solution.py:138
  9.2 0.0 collective-permute-start.5
  9.2 0.0 collective-permute-start
  9.2 2.9 %collective-permute-done.1.refs_5_ = bf16[32,2176]{1,0:T(8,128)(2,1)S(1)} collective-permute-done((bf16[32,2176]{1,0:T(8,128)(2,1)S(1)}, bf16[32,2176]{1,0:T(8,128)(2,1)S(1)}, u32[]{:S(2)}, u32[]{:S(2)}) %collective-permute-start.1) | collective-permute-done | bytes 139296 | tf_op jit(solution)/shard_map/ppermute | solution.py:138
  12.1 0.0 collective-permute-start.2
  12.1 7.9 %collective-permute-done.3.refs_6_ = bf16[32,2176]{1,0:T(8,128)(2,1)S(1)} collective-permute-done((bf16[32,2176]{1,0:T(8,128)(2,1)S(1)}, bf16[32,2176]{1,0:T(8,128)(2,1)S(1)}, u32[]{:S(2)}, u32[]{:S(2)}) %collective-permute-start.3) | collective-permute-done | bytes 139296 | tf_op jit(solution)/shard_map/ppermute | solution.py:138
  20.0 0.0 collective-permute-start.4
  20.0 0.0 collective-permute-done.5.refs_7_
  20.0 0.5 collective-permute-start.6
  20.5 4.7 %fetch_weights.1 = (bf16[2048,1024]{1,0:T(8,128)(2,1)S(1)}, bf16[2048,1024]{1,0:T(8,128)(2,1)S(1)}, bf16[1024,2048]{1,0:T(8,128)(2,1)S(1)}) custom-call(bf16[16,128]{1,0:T(8,128)(2,1)S(1)} %slice.40.tie, bf16[1,2048,1024]{2,1,0:T(8,128)(2,1)} %gate.1, bf16[1,2048,1024]{2,1,0:T(8,128)(2,1)} %up.1, bf16[1,1024,2048]{2,1,0:T(8,128)(2,1)} %down.1), custom_call_target="tpu_custom_call" | custom-call | flops 4000000000 | bytes 12582912 | tf_op jit(solution)/shard_map/fetch_weights/pallas_call | solution.py:57
  25.2 0.0 collective-permute-done.refs_0_
  25.2 0.0 collective-permute-done.2.refs_1_
  25.2 0.0 collective-permute-done.4.refs_2_
  25.2 0.0 collective-permute-done.6.refs_3_
  25.3 0.0 copy-start.2
  25.3 3.6 %expert.1 = (bf16[128,2048]{1,0:T(8,128)(2,1)S(1)}, f32[128,2048]{1,0:T(8,128)S(1)}) custom-call(bf16[32,2176]{1,0:T(8,128)(2,1)S(1)} %collective-permute-done.refs_0_, bf16[32,2176]{1,0:T(8,128)(2,1)S(1)} %collective-permute-done.2.refs_1_, bf16[32,2176]{1,0:T(8,128)(2,1)S(1)} %collective-permute-done.4.refs_2_, ...), custom_call_target="tpu_custom_call" | custom-call | flops 3221225472 | bytes 1048576 | tf_op jit(solution)/shard_map/expert/pallas_call | solution.py:104
  28.8 0.1 collective-permute-start.7
  28.9 0.0 copy-done.2
  28.9 1.1 %fusion.7 = f32[32,512]{1,0:T(8,128)} fusion(bf16[2048,512]{1,0:T(8,128)(2,1)S(1)} %copy-done.2, bf16[32,2176]{1,0:T(8,128)(2,1)S(1)} %prepare.1.refs_4_), kind=kOutput, calls=%fused_computation.14 | convolution fusion | flops 67108864 | bytes 2293760 | tf_op jit(solution)/shard_map/dot_general | solution.py:161
  30.0 0.8 %collective-permute-done.7 = bf16[128,2048]{1,0:T(8,128)(2,1)S(1)} collective-permute-done((bf16[128,2048]{1,0:T(8,128)(2,1)S(1)}, bf16[128,2048]{1,0:T(8,128)(2,1)S(1)}, u32[]{:S(2)}, u32[]{:S(2)}) %collective-permute-start.7) | collective-permute-done | bytes 524320 | tf_op jit(solution)/shard_map/ppermute | solution.py:138
  30.8 0.0 copy-start.3
  30.8 0.9 %add_convert_fusion.2 = (bf16[32,2048]{1,0:T(8,128)(2,1)}, bf16[32,2048]{1,0:T(8,128)(2,1)}, bf16[32,2048]{1,0:T(8,128)(2,1)}) fusion(f32[128,2048]{1,0:T(8,128)S(1)} %get-tuple-element.19, bf16[128,2048]{1,0:T(8,128)(2,1)S(1)} %collective-permute-done.7), kind=kLoop, calls=%fused_computation.8 | loop fusion | flops 589824 | bytes 1572864 | tf_op jit(solution)/shard_map/convert_element_type | solution.py:174
  31.7 2.3 %collective-permute-start.10 = (bf16[32,2048]{1,0:T(8,128)(2,1)}, bf16[32,2048]{1,0:T(8,128)(2,1)}, u32[]{:S(2)}, u32[]{:S(2)}) collective-permute-start(bf16[32,2048]{1,0:T(8,128)(2,1)} %get-tuple-element.26), channel_id=1, source_target_pairs={{0,12},{2,14},{4,8},{6,10},{8,4},{10,6},{12,0},{14,2},{1,13},{3,15... | collective-permute-start | bytes 393224 | tf_op jit(solution)/shard_map/ppermute | solution.py:138
  34.0 1.1 %collective-permute-start.8 = (bf16[32,2048]{1,0:T(8,128)(2,1)}, bf16[32,2048]{1,0:T(8,128)(2,1)}, u32[]{:S(2)}, u32[]{:S(2)}) collective-permute-start(bf16[32,2048]{1,0:T(8,128)(2,1)} %get-tuple-element.25), channel_id=1, source_target_pairs={{0,4},{2,6},{4,0},{6,2},{8,12},{10,14},{12,8},{14,10},{1,5},{3,7},... | collective-permute-start | bytes 393224 | tf_op jit(solution)/shard_map/ppermute | solution.py:138
  35.1 0.0 copy-done.3
  35.1 1.0 %collective-permute-start.9 = (bf16[32,2048]{1,0:T(8,128)(2,1)}, bf16[32,2048]{1,0:T(8,128)(2,1)}, u32[]{:S(2)}, u32[]{:S(2)}) collective-permute-start(bf16[32,2048]{1,0:T(8,128)(2,1)} %get-tuple-element.27), channel_id=1, source_target_pairs={{0,8},{2,10},{4,12},{6,14},{8,0},{10,2},{12,4},{14,6},{1,9},{3,11}... | collective-permute-start | bytes 393224 | tf_op jit(solution)/shard_map/ppermute | solution.py:138
  36.1 0.0 copy-done
  36.1 2.5 %fusion.1 = f32[32,2048]{1,0:T(8,128)S(1)} fusion(bf16[512,2048]{1,0:T(8,128)(2,1)S(1)} %copy-done, bf16[2048,512]{1,0:T(8,128)(2,1)} %param.19, bf16[32,2176]{1,0:T(8,128)(2,1)S(1)} %prepare.1.refs_4_, f32[32,512]{1,0:T(8,128)} %fusion.7), kind=kOutput, calls=%fused_computation.2 | convolution fusion | flops 134316032 | bytes 4653056 | tf_op jit(solution)/shard_map/dot_general | solution.py:164
  38.6 1.6 %collective-permute-done.10 = bf16[32,2048]{1,0:T(8,128)(2,1)} collective-permute-done((bf16[32,2048]{1,0:T(8,128)(2,1)}, bf16[32,2048]{1,0:T(8,128)(2,1)}, u32[]{:S(2)}, u32[]{:S(2)}) %collective-permute-start.10) | collective-permute-done | bytes 131104 | tf_op jit(solution)/shard_map/ppermute | solution.py:138
  40.2 2.3 %collective-permute-done.8 = bf16[32,2048]{1,0:T(8,128)(2,1)} collective-permute-done((bf16[32,2048]{1,0:T(8,128)(2,1)}, bf16[32,2048]{1,0:T(8,128)(2,1)}, u32[]{:S(2)}, u32[]{:S(2)}) %collective-permute-start.8) | collective-permute-done | bytes 131104 | tf_op jit(solution)/shard_map/ppermute | solution.py:138
  42.5 4.9 %collective-permute-done.9 = bf16[32,2048]{1,0:T(8,128)(2,1)} collective-permute-done((bf16[32,2048]{1,0:T(8,128)(2,1)}, bf16[32,2048]{1,0:T(8,128)(2,1)}, u32[]{:S(2)}, u32[]{:S(2)}) %collective-permute-start.9) | collective-permute-done | bytes 131104 | tf_op jit(solution)/shard_map/ppermute | solution.py:138
  47.5 1.2 %fusion.17 = (bf16[32,2048]{1,0:T(8,128)(2,1)S(1)}, f32[32,2048]{1,0:T(8,128)S(1)}) fusion(bf16[32,2048]{1,0:T(8,128)(2,1)} %collective-permute-done.10, bf16[32,2048]{1,0:T(8,128)(2,1)} %collective-permute-done.9, bf16[32,2048]{1,0:T(8,128)(2,1)} %collective-permute-done.8, f32[32,2048]{1,0:T(8,128)S(1)} %fusion.1, bf16[128,2048]{1,0:T(8,128)(2,1)} %copy-done.3, ...), kind=kLoop, calls=%fused_computation.32 | loop fusion | flops 655360 | bytes 1441792 | tf_op jit(solution)/shard_map/convert_element_type | solution.py:177
  48.7 1.6 %collective-permute-start.11 = (bf16[32,2048]{1,0:T(8,128)(2,1)S(1)}, bf16[32,2048]{1,0:T(8,128)(2,1)S(1)}, u32[]{:S(2)}, u32[]{:S(2)}) collective-permute-start(bf16[32,2048]{1,0:T(8,128)(2,1)S(1)} %get-tuple-element.23), channel_id=1, source_target_pairs={{0,1},{1,0},{2,3},{3,2},{4,5},{5,4},{6,7},{7,6},{8,9},{9,8},{10,11... | collective-permute-start | bytes 393224 | tf_op jit(solution)/shard_map/ppermute | solution.py:141
  50.2 0.7 %convert_element_type.69 = f32[1024]{0:T(1024)S(1)} convert(bf16[1024]{0:T(1024)(128)(2,1)} %param.21) | non-fusion elementwise | flops 1024 | bytes 6144 | tf_op jit(solution)/shard_map/convert_element_type | solution.py:185
  50.9 2.9 %collective-permute-done.11 = bf16[32,2048]{1,0:T(8,128)(2,1)S(1)} collective-permute-done((bf16[32,2048]{1,0:T(8,128)(2,1)S(1)}, bf16[32,2048]{1,0:T(8,128)(2,1)S(1)}, u32[]{:S(2)}, u32[]{:S(2)}) %collective-permute-start.11) | collective-permute-done | bytes 131104 | tf_op jit(solution)/shard_map/ppermute | solution.py:141
  53.8 0.2 multiply_reduce_fusion
  54.0 0.7 %fusion.4 = bf16[32,1024]{1,0:T(8,128)(2,1)} fusion(f32[32,2048]{1,0:T(8,128)S(1)} %get-tuple-element.22, f32[1024]{0:T(1024)S(1)} %convert_element_type.69, f32[32]{0:T(128)S(1)} %add_rsqrt_fusion, pred[1024]{0:T(1024)(128)(4,1)S(1)} %slice_reduce_fusion), kind=kLoop, calls=%fused_computation.12 | loop fusion | flops 131072 | bytes 332928 | tf_op jit(solution)/shard_map/convert_element_type | solution.py:185
  (5 shorter events, 0.1 us)
Async XLA Ops:
  0.0 36.1 %copy-start = (bf16[512,2048]{1,0:T(8,128)(2,1)S(1)}, bf16[512,2048]{1,0:T(8,128)(2,1)}, u32[]{:S(2)}) copy-start(bf16[512,2048]{1,0:T(8,128)(2,1)} %param.20) | copy-start | bytes 6291460
  2.4 0.9 %copy-start.1 = (bf16[32,2048]{1,0:T(8,128)(2,1)S(1)}, bf16[32,2048]{1,0:T(8,128)(2,1)}, u32[]{:S(2)}) copy-start(bf16[32,2048]{1,0:T(8,128)(2,1)} %refs_0_.1) | copy-start | bytes 393220
  3.5 8.6 %collective-permute-start.1 = (bf16[32,2176]{1,0:T(8,128)(2,1)S(1)}, bf16[32,2176]{1,0:T(8,128)(2,1)S(1)}, u32[]{:S(2)}, u32[]{:S(2)}) collective-permute-start(bf16[32,2176]{1,0:T(8,128)(2,1)S(1)} %prepare.1.refs_4_), channel_id=1, source_target_pairs={{0,4},{2,6},{4,0},{6,2},{8,12},{10,14},{12,8},{14,10},{1,5},{3,7},... | collective-permute-start | bytes 417800 | tf_op jit(solution)/shard_map/ppermute | solution.py:138
  6.6 13.4 %collective-permute-start.3 = (bf16[32,2176]{1,0:T(8,128)(2,1)S(1)}, bf16[32,2176]{1,0:T(8,128)(2,1)S(1)}, u32[]{:S(2)}, u32[]{:S(2)}) collective-permute-start(bf16[32,2176]{1,0:T(8,128)(2,1)S(1)} %prepare.1.refs_4_), channel_id=1, source_target_pairs={{0,8},{2,10},{4,12},{6,14},{8,0},{10,2},{12,4},{14,6},{1,9},{3,11}... | collective-permute-start | bytes 417800 | tf_op jit(solution)/shard_map/ppermute | solution.py:138
  9.2 10.8 %collective-permute-start.5 = (bf16[32,2176]{1,0:T(8,128)(2,1)S(1)}, bf16[32,2176]{1,0:T(8,128)(2,1)S(1)}, u32[]{:S(2)}, u32[]{:S(2)}) collective-permute-start(bf16[32,2176]{1,0:T(8,128)(2,1)S(1)} %prepare.1.refs_4_), channel_id=1, source_target_pairs={{0,12},{2,14},{4,8},{6,10},{8,4},{10,6},{12,0},{14,2},{1,13},{3,15... | collective-permute-start | bytes 417800 | tf_op jit(solution)/shard_map/ppermute | solution.py:138
  9.2 16.0 %collective-permute-start = (bf16[32,2176]{1,0:T(8,128)(2,1)S(1)}, bf16[32,2176]{1,0:T(8,128)(2,1)S(1)}, u32[]{:S(2)}, u32[]{:S(2)}) collective-permute-start(bf16[32,2176]{1,0:T(8,128)(2,1)S(1)} %prepare.1.refs_4_), channel_id=1, source_target_pairs={{0,2},{2,0},{4,6},{6,4},{8,10},{10,8},{12,14},{14,12},{1,3},{3,1},... | collective-permute-start | bytes 417800 | tf_op jit(solution)/shard_map/ppermute | solution.py:138
  12.1 13.1 %collective-permute-start.2 = (bf16[32,2176]{1,0:T(8,128)(2,1)S(1)}, bf16[32,2176]{1,0:T(8,128)(2,1)S(1)}, u32[]{:S(2)}, u32[]{:S(2)}) collective-permute-start(bf16[32,2176]{1,0:T(8,128)(2,1)S(1)} %collective-permute-done.1.refs_5_), channel_id=1, source_target_pairs={{0,2},{2,0},{4,6},{6,4},{8,10},{10,8},{12,14},{14,12},{1,3},{3,1},... | collective-permute-start | bytes 417800 | tf_op jit(solution)/shard_map/ppermute | solution.py:138
  20.0 5.2 %collective-permute-start.4 = (bf16[32,2176]{1,0:T(8,128)(2,1)S(1)}, bf16[32,2176]{1,0:T(8,128)(2,1)S(1)}, u32[]{:S(2)}, u32[]{:S(2)}) collective-permute-start(bf16[32,2176]{1,0:T(8,128)(2,1)S(1)} %collective-permute-done.3.refs_6_), channel_id=1, source_target_pairs={{0,2},{2,0},{4,6},{6,4},{8,10},{10,8},{12,14},{14,12},{1,3},{3,1},... | collective-permute-start | bytes 417800 | tf_op jit(solution)/shard_map/ppermute | solution.py:138
  20.0 5.2 %collective-permute-start.6 = (bf16[32,2176]{1,0:T(8,128)(2,1)S(1)}, bf16[32,2176]{1,0:T(8,128)(2,1)S(1)}, u32[]{:S(2)}, u32[]{:S(2)}) collective-permute-start(bf16[32,2176]{1,0:T(8,128)(2,1)S(1)} %collective-permute-done.5.refs_7_), channel_id=1, source_target_pairs={{0,2},{2,0},{4,6},{6,4},{8,10},{10,8},{12,14},{14,12},{1,3},{3,1},... | collective-permute-start | bytes 417800 | tf_op jit(solution)/shard_map/ppermute | solution.py:138
  25.3 3.7 %copy-start.2 = (bf16[2048,512]{1,0:T(8,128)(2,1)S(1)}, bf16[2048,512]{1,0:T(8,128)(2,1)}, u32[]{:S(2)}) copy-start(bf16[2048,512]{1,0:T(8,128)(2,1)} %param.18) | copy-start | bytes 6291460
  28.8 2.0 %collective-permute-start.7 = (bf16[128,2048]{1,0:T(8,128)(2,1)S(1)}, bf16[128,2048]{1,0:T(8,128)(2,1)S(1)}, u32[]{:S(2)}, u32[]{:S(2)}) collective-permute-start(bf16[128,2048]{1,0:T(8,128)(2,1)S(1)} %get-tuple-element.20), channel_id=1, source_target_pairs={{0,2},{2,0},{4,6},{6,4},{8,10},{10,8},{12,14},{14,12},{1,3},{3,1},... | collective-permute-start | bytes 1572872 | tf_op jit(solution)/shard_map/ppermute | solution.py:138
  30.8 4.3 %copy-start.3 = (bf16[128,2048]{1,0:T(8,128)(2,1)}, bf16[128,2048]{1,0:T(8,128)(2,1)S(1)}, u32[]{:S(2)}) copy-start(bf16[128,2048]{1,0:T(8,128)(2,1)S(1)} %collective-permute-done.7) | copy-start | bytes 1572868
  31.7 8.5 %collective-permute-start.10 = (bf16[32,2048]{1,0:T(8,128)(2,1)}, bf16[32,2048]{1,0:T(8,128)(2,1)}, u32[]{:S(2)}, u32[]{:S(2)}) collective-permute-start(bf16[32,2048]{1,0:T(8,128)(2,1)} %get-tuple-element.26), channel_id=1, source_target_pairs={{0,12},{2,14},{4,8},{6,10},{8,4},{10,6},{12,0},{14,2},{1,13},{3,15... | collective-permute-start | bytes 393224 | tf_op jit(solution)/shard_map/ppermute | solution.py:138
  34.0 8.6 %collective-permute-start.8 = (bf16[32,2048]{1,0:T(8,128)(2,1)}, bf16[32,2048]{1,0:T(8,128)(2,1)}, u32[]{:S(2)}, u32[]{:S(2)}) collective-permute-start(bf16[32,2048]{1,0:T(8,128)(2,1)} %get-tuple-element.25), channel_id=1, source_target_pairs={{0,4},{2,6},{4,0},{6,2},{8,12},{10,14},{12,8},{14,10},{1,5},{3,7},... | collective-permute-start | bytes 393224 | tf_op jit(solution)/shard_map/ppermute | solution.py:138
  35.1 12.4 %collective-permute-start.9 = (bf16[32,2048]{1,0:T(8,128)(2,1)}, bf16[32,2048]{1,0:T(8,128)(2,1)}, u32[]{:S(2)}, u32[]{:S(2)}) collective-permute-start(bf16[32,2048]{1,0:T(8,128)(2,1)} %get-tuple-element.27), channel_id=1, source_target_pairs={{0,8},{2,10},{4,12},{6,14},{8,0},{10,2},{12,4},{14,6},{1,9},{3,11}... | collective-permute-start | bytes 393224 | tf_op jit(solution)/shard_map/ppermute | solution.py:138
  48.7 5.2 %collective-permute-start.11 = (bf16[32,2048]{1,0:T(8,128)(2,1)S(1)}, bf16[32,2048]{1,0:T(8,128)(2,1)S(1)}, u32[]{:S(2)}, u32[]{:S(2)}) collective-permute-start(bf16[32,2048]{1,0:T(8,128)(2,1)S(1)} %get-tuple-element.23), channel_id=1, source_target_pairs={{0,1},{1,0},{2,3},{3,2},{4,5},{5,4},{6,7},{7,6},{8,9},{9,8},{10,11... | collective-permute-start | bytes 393224 | tf_op jit(solution)/shard_map/ppermute | solution.py:141
